TPU v7x, 256 devices: a whole 4x4x8 slice. The times are simulated.
256 devices in a mesh: sp: 32 (over z, x), fs: 4 (over y), tp: 2 (over core).
Axes of the slice: x: 4, y: 4, z: 8, core: 2. Of those that a mesh axis runs over, the one named last changes fastest.
Arguments:
- tokens: bfloat16 [4, 8192, 2048], P('fs', 'sp', 'tp'), may hold values from -6 to 6
- norm_gain: float32 [2048], replicated, may hold values from 0.1 to 1.9
- query_weight: bfloat16 [2048, 1024], P(('sp', 'fs'), 'tp'), may hold values from -0.125 to 0.125
- forget_weight: bfloat16 [2048, 1024], P(('sp', 'fs'), 'tp'), may hold values from -0.125 to 0.125
- value_weight: bfloat16 [2048, 1024], P(('sp', 'fs'), 'tp'), may hold values from -0.125 to 0.125
- outgate_weight: bfloat16 [2048, 1024], P(('sp', 'fs'), 'tp'), may hold values from -0.125 to 0.125
- pool_in_weight: bfloat16 [2048, 1024], P(('sp', 'fs'), 'tp'), may hold values from -0.125 to 0.125
- forget_room: float32 [1024], P('tp'), may hold values from 0 to 0.06
- decay_shift: float32 [4, 8192, 8], P('fs', 'sp', 'tp'), may hold values from -0.6 to 0
- head_gain: float32 [128], replicated, may hold values from 0.1 to 1.9
- start_state: float32 [4, 8, 128, 128], P('fs', 'tp'), may hold values from -0.03314563 to 0.03314563
- pool_map: bfloat16 [4, 256, 256], P('tp'), may hold values from -0.375 to 0.375
- pool_scale: float32 [1024], P('tp'), may hold values from 0.1 to 1.9
- out_rec_weight: bfloat16 [1024, 2048], P('tp', ('sp', 'fs')), may hold values from -0.125 to 0.125
- out_pool_weight: bfloat16 [1024, 2048], P('tp', ('sp', 'fs')), may hold values from -0.125 to 0.125
Outputs:
- mixed: bfloat16 [4, 8192, 2048], P('fs', ('sp', 'tp'))
All inputs are finite; a program needn't handle non-finite values.
Results may differ from a plain program's by a relative error of at most 0.013.
Values may be sent and summed in bfloat16 or wider, within the bound.
A program may use at most 128 MiB of HBM per device.

v0:
```python
import jax
import jax.numpy as jnp
from jax import lax
from jax.sharding import Mesh
from jax.sharding import PartitionSpec as P

HEAD = 128
POOL_DIM = 256
WIDEST = 16
BLOCK = 128
SP_FS = ("sp_0", "sp_1", "fs")
SP = ("sp_0", "sp_1")
SP_TP = ("sp_0", "sp_1", "tp")


EPSILON = 1e-06


def from_everyone(array, axis):
    count = lax.axis_size(axis)
    return lax.all_to_all(
        jnp.broadcast_to(array[None], (count, *array.shape)), axis, 0, 0, tiled=True
    )


def laid_out(blocks, dim):
    blocks = jnp.moveaxis(blocks, 0, dim)
    lengths = blocks.shape
    return blocks.reshape(*lengths[:dim], lengths[dim] * lengths[dim + 1], *lengths[dim + 2 :])


def gather_directly(array, axis, dim):
    blocks = from_everyone(array, axis)
    return laid_out(blocks, dim)


def gather_turned(arrays, axis, dims):
    turned = [jnp.moveaxis(a, dim, 0) for a, dim in zip(arrays, dims)]
    both = jnp.concatenate([t.reshape(len(t), -1) for t in turned], axis=1)
    filled, at, done = (lax.all_gather(both, axis, axis=0, tiled=True), 0, [])
    for t, dim in zip(turned, dims):
        slab = filled[:, at : at + t[0].size].reshape(-1, *t.shape[1:])
        done.append(jnp.moveaxis(slab, 0, dim))
        at += t[0].size
    return tuple(done)


def neutral_like(array, identity):
    return jax.tree.map(
        lambda part, zero: jnp.zeros_like(part) + jnp.asarray(zero, part.dtype), array, identity
    )


def entering_2(array, axes, combine, identity):
    before = start = neutral_like(array, identity)
    so_far = array
    for axis in reversed(axes):
        count, mine = (lax.axis_size(axis), lax.axis_index(axis))
        pieces = jax.tree.map(
            lambda part, kind: lax.all_gather(part.astype(kind), axis),
            so_far,
            (jnp.bfloat16, jnp.bfloat16),
        )
        inside, so_far = (start, start)
        for k in range(count):
            passed = k < mine
            so_far = combine(
                so_far, jax.tree.map(lambda part, own: part[k].astype(own.dtype), pieces, array)
            )
            inside = jax.tree.map(lambda new, old: jnp.where(passed, new, old), so_far, inside)
        before = combine(inside, before)
    return before


def shifted(value, axis, steps):
    count = lax.axis_size(axis)
    first, last = (max(0, -steps), min(count, count - steps))
    return lax.ppermute(value, axis, [(source, source + steps) for source in range(first, last)])


def in_blocks(array, dim, count):
    lengths = array.shape
    blocks = array.reshape(*lengths[:dim], count, lengths[dim] // count, *lengths[dim + 1 :])
    return jnp.moveaxis(blocks, dim, 0)


def sum_at_owner(array, axis, dim):
    blocks = in_blocks(array, dim, lax.axis_size(axis))
    arrived = lax.all_to_all(blocks, axis, split_axis=0, concat_axis=0, tiled=True)
    return arrived.astype(jnp.float32).sum(axis=0)


def rms_scale(entry_vectors):
    return lax.rsqrt(jnp.mean(entry_vectors * entry_vectors, axis=-1, keepdims=True) + EPSILON)


def compose(earlier, later):
    return (earlier[0] + later[0], jnp.exp(later[0])[:, :, None] * earlier[1] + later[1])


def per_device(
    tokens,
    norm_gain,
    query_weight,
    forget_weight,
    value_weight,
    outgate_weight,
    pool_in_weight,
    forget_room,
    decay_shift,
    head_gain,
    start_state,
    pool_map,
    pool_scale,
    out_rec_weight,
    out_pool_weight,
):
    widened = gather_directly(tokens, "tp", 2)[0].astype(jnp.float32)
    rescaled_input = (widened * rms_scale(widened) * norm_gain).astype(jnp.bfloat16)
    out_local = jnp.concatenate([out_rec_weight, out_pool_weight], axis=0)
    gathered = gather_turned(
        (query_weight, forget_weight, value_weight, outgate_weight, pool_in_weight, out_local),
        SP_FS,
        (0, 0, 0, 0, 0, 1),
    )
    projected = [
        jnp.dot(rescaled_input, weight, preferred_element_type=jnp.float32).astype(jnp.bfloat16)
        for weight in gathered[:5]
    ]
    length = rescaled_input.shape[0]
    head_count = forget_room.shape[0] // HEAD
    blocks = length // BLOCK
    queries = jax.nn.silu(projected[0].astype(jnp.float32)) * HEAD ** (-0.5)
    keyed = forget_room[None, :] * (1.0 - jax.nn.sigmoid(projected[1].astype(jnp.float32)))
    log_decay = jnp.log1p(-keyed).reshape(length, head_count, HEAD) + decay_shift[0][:, :, None]

    def to_blocks(entry_vectors):
        return entry_vectors.reshape(blocks, BLOCK, head_count, HEAD).transpose(2, 0, 1, 3)

    query_blocks = to_blocks(queries)
    key_blocks = to_blocks(keyed)
    value_blocks = to_blocks(projected[2])
    within = jnp.cumsum(to_blocks(log_decay), axis=2)
    centre = within[:, :, BLOCK // 2 - 1 : BLOCK // 2]
    ending = within[:, :, BLOCK - 1 : BLOCK]
    causal = jnp.tril(jnp.ones((BLOCK, BLOCK), jnp.float32))
    scores = (
        jnp.einsum(
            "hncd,hnsd->hncs",
            (query_blocks * jnp.exp(within - centre)).astype(jnp.bfloat16),
            (key_blocks * jnp.exp(centre - within)).astype(jnp.bfloat16),
            preferred_element_type=jnp.float32,
        )
        * causal
    )
    inside = jnp.einsum(
        "hncs,hnse->hnce",
        scores.astype(jnp.bfloat16),
        value_blocks,
        preferred_element_type=jnp.float32,
    )
    added = jnp.einsum(
        "hncd,hnce->nhde",
        (key_blocks * jnp.exp(ending - within)).astype(jnp.bfloat16),
        value_blocks,
        preferred_element_type=jnp.float32,
    )
    block_decay = ending[:, :, 0, :].transpose(1, 0, 2)

    def advance(memory, inputs):
        decay_piece, added_piece = inputs
        return (jnp.exp(decay_piece)[:, :, None] * memory + added_piece, memory)

    local_state, block_starts = lax.scan(
        advance, jnp.zeros((head_count, HEAD, HEAD), jnp.float32), (block_decay, added)
    )
    decay_before = jnp.cumsum(block_decay, axis=0) - block_decay
    local_decay = jnp.sum(block_decay, axis=0)
    identity = (jnp.zeros_like(local_decay), jnp.zeros_like(local_state))
    prefix_decay, prefix_state = entering_2((local_decay, local_state), SP, compose, identity)
    entering = prefix_state + jnp.exp(prefix_decay)[:, :, None] * start_state[0]
    block_states = block_starts + jnp.exp(decay_before)[:, :, :, None] * entering[None]
    carried = jnp.einsum(
        "hncd,nhde->hnce",
        (query_blocks * jnp.exp(within)).astype(jnp.bfloat16),
        block_states.astype(jnp.bfloat16),
        preferred_element_type=jnp.float32,
    )
    outputs = (inside + carried).transpose(1, 2, 0, 3).reshape(length, head_count, HEAD)
    gating = jax.nn.silu(projected[3].astype(jnp.float32)).reshape(length, head_count, HEAD)
    rec_out = (outputs * rms_scale(outputs) * head_gain * gating).reshape(length, head_count * HEAD)
    rec_out = rec_out.astype(jnp.bfloat16)
    pool_input = projected[4]
    columns = pool_input.shape[1]
    border = shifted(pool_input[length - WIDEST :], SP, 1)
    extended = jnp.concatenate([border, pool_input], axis=0).astype(jnp.float32)
    feature_lane = lax.axis_index("tp") * columns + jnp.arange(columns, dtype=jnp.int32)
    reach = jnp.left_shift(jnp.int32(2), feature_lane // POOL_DIM)
    window_sum = jnp.zeros((length, columns), jnp.float32)
    for offset in range(WIDEST):
        window_sum = window_sum + extended[WIDEST - offset : WIDEST - offset + length] * (
            offset < reach
        ).astype(jnp.float32)
    position = lax.axis_index(SP) * length + jnp.arange(length, dtype=jnp.int32)
    amount = jnp.minimum(position[:, None] + 1, reach[None, :]).astype(jnp.float32)
    pooled = (window_sum / amount - extended[WIDEST:]).astype(jnp.bfloat16)
    group_count = pool_map.shape[0]
    mapped = jnp.einsum(
        "tgc,gcd->tgd",
        pooled.reshape(length, group_count, POOL_DIM),
        pool_map,
        preferred_element_type=jnp.float32,
    )
    pool_out = (mapped.reshape(length, columns) * pool_scale).astype(jnp.bfloat16)
    joined = jnp.concatenate([rec_out, pool_out], axis=1)
    out_whole = gathered[5]
    mixed_rows = sum_at_owner(
        jnp.dot(joined, out_whole, preferred_element_type=jnp.float32).astype(jnp.bfloat16), "tp", 0
    )
    return mixed_rows.astype(jnp.bfloat16)[None]


def solution(mesh):
    finer = Mesh(
        mesh.devices.reshape(8, 4, mesh.shape["fs"], mesh.shape["tp"]), ("sp_0", "sp_1", "fs", "tp")
    )
    placed = (
        P("fs", SP, "tp"),
        P(),
        P(SP_FS, "tp"),
        P(SP_FS, "tp"),
        P(SP_FS, "tp"),
        P(SP_FS, "tp"),
        P(SP_FS, "tp"),
        P("tp"),
        P("fs", SP, "tp"),
        P(),
        P("fs", "tp", None, None),
        P("tp", None, None),
        P("tp"),
        P("tp", SP_FS),
        P("tp", SP_FS),
    )
    return jax.shard_map(
        per_device, mesh=finer, in_specs=placed, out_specs=P("fs", SP_TP, None), check_vma=False
    )
```

profile of v0, /device:TPU:1, one launch (start us, length us, event | category | flops | bytes accessed | tf_op | source)
XLA Modules:
  0.0 264.8 jit_solution(8559160675575011905)
XLA Ops:
  6.5 0.8 constant_dynamic-update-slice_fusion.4
  7.3 0.7 constant_dynamic-update-slice_fusion.3
  8.0 0.7 constant_dynamic-update-slice_fusion.2
  8.7 0.7 constant_dynamic-update-slice_fusion.1
  9.5 0.7 constant_dynamic-update-slice_fusion
  10.2 0.7 fusion.123
  10.9 0.6 copy-done.3
  11.6 1.2 copy.43
  12.9 1.1 broadcast_in_dim.22
  13.9 6.8 %all-to-all-start = ((bf16[2,1,256,1024]{2,3,1,0:T(8,128)(2,1)}), bf16[2,1,256,1024]{2,3,1,0:T(8,128)(2,1)S(1)}, u32[]{:S(2)}, u32[]{:S(2)}) async-start(bf16[2,1,256,1024]{2,3,1,0:T(8,128)(2,1)} %broadcast_in_dim.22), calls=%async_computation | async-start | bytes 2097152 | tf_op jit(solution)/shard_map/all_to_all | solution.py:21
  20.7 0.6 add_add_fusion
  21.4 0.6 compare_convert_fusion.4
  21.9 0.6 compare_convert_fusion.6
  22.5 0.6 compare_convert_fusion.8
  23.2 0.6 compare_convert_fusion.10
  23.8 0.6 compare_convert_fusion.12
  24.4 0.6 compare_convert_fusion.14
  25.0 0.3 multiply_reduce_fusion
  25.3 0.6 broadcast_bitcast_fusion
  26.1 0.3 fusion.16
  26.4 131.7 %all-gather.6.cloned.1.call-done = bf16[2048,3584]{1,0:T(8,128)(2,1)} async-done(((bf16[16,3584]{1,0:T(8,128)(2,1)}), bf16[2048,3584]{1,0:T(8,128)(2,1)}) %all-gather.6.cloned.1.call-update) | async-done | bytes 14680080 | tf_op jit(solution)/shard_map/all_gather | solution.py:40
  158.1 2.5 negate_log-plus-one_fusion
  161.1 0.5 reduce_window_sum.22
  161.6 7.6 %all-gather.2 = bf16[4,4,128]{2,1,0:T(4,128)(2,1)S(1)} all-gather(bf16[1,4,128]{2,1,0:T(4,128)(2,1)S(1)} %bitcast.212), channel_id=2, replica_groups=mesh['sp_0'=8,'sp_1'=4,'fs'=4,'tp'=2] {'sp_1'}, dimensions={0}, use_global_device_ids=true | all-gather | bytes 5120 | tf_op jit(solution)/shard_map/all_gather | solution.py:60
  169.3 11.1 %all_gather.23 = bf16[8,4,128]{2,1,0:T(4,128)(2,1)S(1)} all-gather(bf16[1,4,128]{2,1,0:T(4,128)(2,1)S(1)} %get-tuple-element.93), channel_id=1, replica_groups=mesh['sp_0'=8,'sp_1'=4,'fs'=4,'tp'=2] {'sp_0'}, dimensions={0}, use_global_device_ids=true | all-gather | bytes 9216 | tf_op jit(solution)/shard_map/all_gather | solution.py:60
  180.6 2.3 fusion.24
  183.0 0.3 fusion.112
  183.3 1.9 while.13
  183.3 0.7 bitcast_dynamic-update-slice_fusion.2
  184.2 0.7 bitcast_dynamic-update-slice_fusion.2
  185.2 9.9 %all-gather.1 = bf16[16,128,128]{2,1,0:T(8,128)(2,1)S(1)} all-gather(bf16[4,128,128]{2,1,0:T(8,128)(2,1)S(1)} %convert_element_type.456), channel_id=3, replica_groups=mesh['sp_0'=8,'sp_1'=4,'fs'=4,'tp'=2] {'sp_1'}, dimensions={0}, use_global_device_ids=true | all-gather | bytes 655360 | tf_op jit(solution)/shard_map/all_gather | solution.py:60
  195.1 0.6 exponential_bitcast_fusion.1
  195.7 1.0 fusion.118
  196.7 2.7 %multiply_multiply_fusion = f32[256,512]{1,0:T(8,128)S(1)} fusion(bf16[256,2048]{0,1:T(8,128)(2,1)} %copy-done.1, bf16[2048,3584]{1,0:T(8,128)(2,1)} %all-gather.6.cloned.1.call-done), kind=kOutput, calls=%fused_computation.94 | convolution fusion | flops 537788416 | bytes 3670016 | tf_op jit(solution)/shard_map/dot_general | solution.py:127
  199.6 2.6 fusion.30
  202.4 1.3 collective-permute-start
  203.7 1.3 fusion.61
  205.2 1.0 fusion.94
  206.3 0.3 fusion.100
  206.9 29.0 %all-gather.8.cloned.1.call-done = bf16[8,4,128,128]{3,2,1,0:T(8,128)(2,1)} async-done(((bf16[1,4,128,128]{3,2,1,0:T(8,128)(2,1)}), bf16[8,4,128,128]{3,2,1,0:T(8,128)(2,1)}) %all-gather.8.cloned.1.call-update) | async-done | bytes 1048592 | tf_op jit(solution)/shard_map/all_gather | solution.py:60
  236.0 2.2 fusion.110
  238.2 1.7 multiply_reduce_fusion.1
  240.1 0.2 copy.54
  240.4 0.3 mul.448
  240.7 2.7 %fusion.64 = bf16[256,512]{1,0:T(8,128)(2,1)S(1)} fusion(f32[32,8,4,128]{3,2,1,0:T(4,128)S(1)} %bitcast.202, f32[32,8,4,128]{3,2,1,0:T(4,128)S(1)} %bitcast.205, bf16[256,2048]{0,1:T(8,128)(2,1)} %copy-done.1, bf16[2048,3584]{1,0:T(8,128)(2,1)} %all-gather.6.cloned.1.call-done, f32[512]{0:T(512)S(1)} %copy-done.19), kind=kOutput, calls=%fused_computation.44 | convolution fusion | flops 538181632 | bytes 4458496 | tf_op jit(solution)/shard_map/dot_general | solution.py:127
  243.4 3.5 %fusion.2 = bf16[256,2048]{1,0:T(8,128)(2,1)S(1)} fusion(bf16[2048,3584]{1,0:T(8,128)(2,1)} %all-gather.6.cloned.1.call-done, bf16[256,512]{1,0:T(8,128)(2,1)S(1)} %multiply_convert_fusion, bf16[256,512]{1,0:T(8,128)(2,1)S(1)} %fusion.64), kind=kOutput, calls=%fused_computation.6 | convolution fusion | flops 1075314688 | bytes 5767168 | tf_op jit(solution)/shard_map/dot_general | solution.py:218
  246.9 9.9 %all_to_all.10 = bf16[2,128,2048]{2,1,0:T(8,128)(2,1)S(1)} all-to-all(bf16[2,128,2048]{2,1,0:T(8,128)(2,1)S(1)} %bitcast.200), channel_id=1, replica_groups=mesh['sp_0'=8,'sp_1'=4,'fs'=4,'tp'=2] {'tp'}, dimensions={0} | all-to-all | bytes 2097152 | tf_op jit(solution)/shard_map/all_to_all | solution.py:89
  256.8 1.1 reduce_sum.42
  (85 shorter events, 2.3 us)
Async XLA Ops:
  6.5 199.7 %copy-start = (bf16[2,256,256]{2,1,0:T(8,128)(2,1)S(1)}, bf16[2,256,256]{2,1,0:T(8,128)(2,1)}, u32[]{:S(2)}) copy-start(bf16[2,256,256]{2,1,0:T(8,128)(2,1)} %param.28) | copy-start | bytes 786436
  6.5 151.6 %all-gather.6.cloned.1.call-start = ((), (), s32[]{:S(2)}) async-start(), calls=%async_computation.2 | async-start | bytes 14794752 | tf_op jit(solution)/shard_map/all_gather | solution.py:40
  10.9 0.6 copy-start.3
  12.8 7.9 %copy-start.17 = (f32[1,256,4]{1,2,0:T(4,128)S(1)}, f32[1,256,4]{1,2,0:T(4,128)}, u32[]{:S(2)}) copy-start(f32[1,256,4]{1,2,0:T(4,128)} %param.25) | copy-start | bytes 12292
  12.8 12.5 %copy-start.21 = (f32[128]{0:T(128)S(1)}, f32[128]{0:T(128)}, u32[]{:S(2)}) copy-start(f32[128]{0:T(128)} %param.26) | copy-start | bytes 1540
  13.9 11.1 %all-to-all-start = ((bf16[2,1,256,1024]{2,3,1,0:T(8,128)(2,1)}), bf16[2,1,256,1024]{2,3,1,0:T(8,128)(2,1)S(1)}, u32[]{:S(2)}, u32[]{:S(2)}) async-start(bf16[2,1,256,1024]{2,3,1,0:T(8,128)(2,1)} %broadcast_in_dim.22), calls=%async_computation | async-start | bytes 2097152 | tf_op jit(solution)/shard_map/all_to_all | solution.py:21
  20.7 215.2 %all-gather.8.cloned.1.call-start = ((), (), s32[]{:S(2)}) async-start(), calls=%async_computation.3 | async-start | bytes 1179648 | tf_op jit(solution)/shard_map/all_gather | solution.py:60
  25.0 1.1 copy-start.4
  26.1 132.0 %copy-start.22 = (f32[512]{0:T(512)S(1)}, f32[512]{0:T(512)}, u32[]{:S(2)}) copy-start(f32[512]{0:T(512)} %param.24) | copy-start | bytes 6148
  26.4 154.1 %copy-start.1 = (bf16[256,2048]{0,1:T(8,128)(2,1)}, bf16[256,2048]{0,1:T(8,128)(2,1)S(1)}, u32[]{:S(2)}) copy-start(bf16[256,2048]{0,1:T(8,128)(2,1)S(1)} %fusion.16) | copy-start | bytes 3145732
  202.3 2.8 %copy-start.5 = (f32[512]{0:T(512)S(1)}, f32[512]{0:T(512)}, u32[]{:S(2)}) copy-start(f32[512]{0:T(512)} %get-tuple-element.107) | copy-start | bytes 6148
  202.3 2.8 %copy-start.6 = (f32[512]{0:T(512)S(1)}, f32[512]{0:T(512)}, u32[]{:S(2)}) copy-start(f32[512]{0:T(512)} %get-tuple-element.108) | copy-start | bytes 6148
  202.3 2.8 %copy-start.7 = (f32[512]{0:T(512)S(1)}, f32[512]{0:T(512)}, u32[]{:S(2)}) copy-start(f32[512]{0:T(512)} %get-tuple-element.109) | copy-start | bytes 6148
  202.3 2.8 %copy-start.8 = (f32[512]{0:T(512)S(1)}, f32[512]{0:T(512)}, u32[]{:S(2)}) copy-start(f32[512]{0:T(512)} %get-tuple-element.110) | copy-start | bytes 6148
  202.3 2.8 %copy-start.9 = (f32[512]{0:T(512)S(1)}, f32[512]{0:T(512)}, u32[]{:S(2)}) copy-start(f32[512]{0:T(512)} %get-tuple-element.111) | copy-start | bytes 6148
  202.3 2.8 %copy-start.10 = (f32[512]{0:T(512)S(1)}, f32[512]{0:T(512)}, u32[]{:S(2)}) copy-start(f32[512]{0:T(512)} %get-tuple-element.112) | copy-start | bytes 6148
  202.3 2.8 %copy-start.11 = (f32[512]{0:T(512)S(1)}, f32[512]{0:T(512)}, u32[]{:S(2)}) copy-start(f32[512]{0:T(512)} %get-tuple-element.113) | copy-start | bytes 6148
  202.3 2.8 %copy-start.12 = (f32[512]{0:T(512)S(1)}, f32[512]{0:T(512)}, u32[]{:S(2)}) copy-start(f32[512]{0:T(512)} %get-tuple-element.114) | copy-start | bytes 6148
  202.3 2.8 %copy-start.13 = (f32[512]{0:T(512)S(1)}, f32[512]{0:T(512)}, u32[]{:S(2)}) copy-start(f32[512]{0:T(512)} %get-tuple-element.115) | copy-start | bytes 6148
  202.4 2.8 %copy-start.14 = (f32[512]{0:T(512)S(1)}, f32[512]{0:T(512)}, u32[]{:S(2)}) copy-start(f32[512]{0:T(512)} %get-tuple-element.116) | copy-start | bytes 6148
  202.4 2.8 %copy-start.15 = (f32[512]{0:T(512)S(1)}, f32[512]{0:T(512)}, u32[]{:S(2)}) copy-start(f32[512]{0:T(512)} %get-tuple-element.117) | copy-start | bytes 6148
  202.4 2.8 %copy-start.20 = (s32[256]{0:T(256)S(1)}, s32[256]{0:T(256)}, u32[]{:S(2)}) copy-start(s32[256]{0:T(256)} %add_add_fusion) | copy-start | bytes 3076
  202.4 2.6 collective-permute-start
  206.2 0.7 copy-start.18
  206.2 29.7 %copy-start.2 = (f32[1,4,128,128]{3,2,1,0:T(8,128)S(1)}, f32[1,4,128,128]{3,2,1,0:T(8,128)}, u32[]{:S(2)}) copy-start(f32[1,4,128,128]{3,2,1,0:T(8,128)} %param.27) | copy-start | bytes 786436
  206.2 29.7 %copy-start.16 = (f32[4,128]{1,0:T(4,128)S(1)}, f32[4,128]{1,0:T(4,128)}, u32[]{:S(2)}) copy-start(f32[4,128]{1,0:T(4,128)} %get-tuple-element.78) | copy-start | bytes 6148
  238.2 2.5 copy-start.19
Sparse Core Ops, SparseCore 0:
  11.7 146.3 all-gather.5
  196.8 39.0 all-gather.7
where the time goes:
time: 266 us; the launch traced here: 265 us
  waiting for transfers between devices  161 us (61%)
  blocking collectives  38.6 us (15%)
  matrix products  20 us (8%)
  other arithmetic  14.4 us (5%)
  between operations  14 us (5%)
  local copies, waits for them, and re-layouts  9.02 us (3%)
  starting transfers between devices  8.06 us (3%)
    all_gather x1, waiting for transfers between devices, gather_turned(): filled, at, done = (lax.all_gather(both, axis, axis=0, tiled=True), 0, [])  132 us
    all_gather x1, waiting for transfers between devices, entering_2(): lax.all_gather(part.astype(kind), axis)  29 us
    all_gather x3, blocking collectives, entering_2(): lax.all_gather(part.astype(kind), axis)  28.7 us
    dot_general x5, matrix products, per_device(): jnp.dot(rescaled_input, weight, preferred_element_type=jnp.float32)  12.9 us
    all_to_all x1, blocking collectives, sum_at_owner(): lax.all_to_all(blocks, axis, split_axis=0, concat_axis=0, tiled=True)  9.93 us
    all_to_all x1, starting transfers between devices, from_everyone(): lax.all_to_all(jnp.broadcast_to(array[None], (count, *array.shape)), axis...  6.77 us
  transfers between devices with their start and end apart: 4, of which 2 were waited for; matrix products, arithmetic and copies ran while one was open for 6% of the time, Pallas kernels for 0%

commit v1 on v0

v1 whole, which is shorter than its diff:
```python
import jax
import jax.numpy as jnp
from jax import lax
from jax.experimental import pallas as pl
from jax.experimental.pallas import tpu as pltpu
from jax.sharding import Mesh
from jax.sharding import PartitionSpec as P

HEAD = 128
POOL_DIM = 256
BLOCK = 128
SP_FS = ("sp_0", "sp_1", "fs")
SP = ("sp_0", "sp_1")
SP_TP = ("sp_0", "sp_1", "tp")
EPSILON = 1e-06
MESH = pl.DeviceIdType.MESH
NSEM = 160
NZ, NX, NF = 8, 4, 4
WX1, WZ1, WX2, WZ2 = 256, 384, 384, 640
F32, BF16 = jnp.float32, jnp.bfloat16
NT = (((1,), (1,)), ((), ()))
TN = (((0,), (0,)), ((), ()))


def dot(a, b, dims=(((1,), (0,)), ((), ()))):
    return lax.dot_general(a, b, dims, preferred_element_type=F32)


def pack_state(state, decay):
    high = decay.astype(BF16).astype(F32)
    rest = decay - high
    mid = rest.astype(BF16).astype(F32)
    low = rest - mid
    row = lax.broadcasted_iota(jnp.int32, (16, HEAD), 0)
    tail = jnp.where(row == 0, high, jnp.where(row == 1, mid, jnp.where(row == 2, low, 0.0)))
    return jnp.concatenate([state, tail], axis=0).astype(BF16)


def unpack_state(packed):
    whole = packed.astype(F32)
    decay = jnp.sum(whole[HEAD : HEAD + 16], axis=0, keepdims=True)
    return whole[:HEAD], decay


def kernel(
    tok,
    ix1,
    iz1,
    ix2,
    iz2,
    room,
    shift,
    hgain,
    start,
    out,
    T,
    GX1,
    GZ1,
    GX2,
    GZ2,
    SH,
    ST,
    K,
    V,
    Q,
    G,
    C,
    QE,
    INS,
    A0,
    SL,
    SR,
    ZS,
    ZR,
    ES,
    ER,
    EXT,
    BS,
    BR,
    RO,
    PO,
    ACT,
    PS,
    PR,
    send_sems,
    recv_sems,
):
    z, x = lax.axis_index("sp_0"), lax.axis_index("sp_1")
    f, c = lax.axis_index("fs"), lax.axis_index("tp")
    zat = lambda k: lax.rem(z + (k + NZ), NZ)
    xat = lambda k: lax.rem(x + (k + NX), NX)
    fat = lambda k: lax.rem(f + (k + NF), NF)
    other = 1 - c
    here = z * NX + x
    after = lax.rem(here + 1, NZ * NX)
    ahead = lax.rem(here + NZ * NX - 1, NZ * NX)
    nxt = {"sp_0": after // NX, "sp_1": lax.rem(after, NX)}
    prv = {"sp_0": ahead // NX, "sp_1": lax.rem(ahead, NX)}

    barrier = pltpu.get_barrier_semaphore()
    met = [{"tp": other}, nxt, prv]
    met += [{"fs": fat(k)} for k in (1, 2, 3)] + [{"sp_1": xat(k)} for k in (1, 2, 3)]
    met += [{"sp_0": zat(k)} for k in range(1, NZ)]
    for who in met:
        pl.semaphore_signal(barrier, inc=1, device_id=who, device_id_type=MESH)

    count = [0]
    sent = []

    def sem():
        count[0] += 1
        assert count[0] <= NSEM
        return count[0] - 1

    def copy(n, src, dst, who):
        return pltpu.make_async_remote_copy(
            src_ref=src,
            dst_ref=dst,
            send_sem=send_sems.at[n],
            recv_sem=recv_sems.at[n],
            device_id=who,
            device_id_type=MESH,
        )

    def send(n, src, dst, who):
        made = copy(n, src, dst, who)
        made.start()
        sent.append(made)

    def landed(n, dst, who):
        copy(n, dst, dst, who).wait_recv()

    mine = pl.ds(pl.multiple_of(f * 16, 16), 16)
    for buffer, own in ((GX1, ix1), (GZ1, iz1), (GX2, ix2), (GZ2, iz2)):
        buffer[z, x, mine, :] = own[f]
    T[c, f] = tok[...]
    SH[f] = shift[...]

    pl.semaphore_wait(barrier, len(met))

    def over_y(pairs):
        waits = []
        for k in (1, 3, 2):
            to = fat(k)
            for buffer, own in pairs:
                n = sem()
                send(n, own.at[to], buffer.at[z, x, mine, :], {"fs": to})
                theirs = pl.ds(pl.multiple_of(fat(-k) * 16, 16), 16)
                waits.append((n, buffer.at[z, x, theirs, :], {"fs": to}))
        return waits

    y1 = over_y(((GX1, ix1), (GZ1, iz1)))
    shift_waits = []
    for k in (1, 3, 2):
        n = sem()
        send(n, shift, SH.at[f], {"fs": fat(k)})
        shift_waits.append((n, SH.at[fat(-k)], {"fs": fat(k)}))

    first, second = pl.ds(0, 128), pl.ds(128, 128)
    relay_waits = []

    def relay(seq, rows):
        n = sem()
        send(n, T.at[c, seq, rows, :], T.at[c, seq, rows, :], {"tp": other})
        relay_waits.append((n, T.at[other, seq, rows, :], {"tp": other}))

    right, left = {"fs": fat(1)}, {"fs": fat(3)}
    tr = [sem(), sem(), sem()]
    tl = [sem(), sem(), sem()]
    for i, (a, b) in enumerate(((first, second), (second, first))):
        send(tr[i], tok.at[a, :], T.at[c, f, a, :], right)
        send(tl[i], tok.at[b, :], T.at[c, f, b, :], left)
    n = sem()
    send(n, tok, T.at[c, f], {"tp": other})
    relay_waits.append((n, T.at[other, f], {"tp": other}))

    def token_steps():
        landed(tr[0], T.at[c, fat(-1), first, :], right)
        send(tr[2], T.at[c, fat(-1), first, :], T.at[c, fat(-1), first, :], right)
        relay(fat(-1), first)
        landed(tl[0], T.at[c, fat(1), second, :], left)
        send(tl[2], T.at[c, fat(1), second, :], T.at[c, fat(1), second, :], left)
        relay(fat(1), second)
        yield
        landed(tr[1], T.at[c, fat(-1), second, :], right)
        relay(fat(-1), second)
        landed(tl[1], T.at[c, fat(1), first, :], left)
        relay(fat(1), first)
        yield
        landed(tr[2], T.at[c, fat(-2), first, :], right)
        relay(fat(-2), first)
        landed(tl[2], T.at[c, fat(2), second, :], left)
        relay(fat(2), second)
        yield

    def plane(GX, GZ, waits):
        zr, zl = {"sp_0": zat(1)}, {"sp_0": zat(-1)}
        xr, xl = {"sp_1": xat(1)}, {"sp_1": xat(-1)}
        low, high = pl.ds(0, 32), pl.ds(32, 32)
        lowx, highx = pl.ds(0, 2), pl.ds(2, 2)
        for w in waits:
            landed(*w)
        xs = []
        for k in (1, 3, 2):
            n = sem()
            send(n, GX.at[z, x], GX.at[z, x], {"sp_1": xat(k)})
            xs.append((n, GX.at[z, xat(-k)], {"sp_1": xat(k)}))
        nr, nl = [sem() for _ in range(4)], [sem() for _ in range(4)]
        send(nr[0], GZ.at[z, x], GZ.at[z, x], zr)
        send(nl[0], GZ.at[z, x], GZ.at[z, x], zl)
        forwards = []
        last = []

        def spread(offset):
            at = zat(offset)
            a, b, e = sem(), sem(), sem()
            send(a, GZ.at[at, x], GZ.at[at, x], xr)
            send(b, GZ.at[at, x], GZ.at[at, x], xl)
            forwards.append((offset, a, b, e))

        def forward():
            for offset, a, b, e in forwards:
                at = zat(offset)
                landed(a, GZ.at[at, xat(-1)], xr)
                if 0 <= offset < 4:
                    send(e, GZ.at[at, xat(-1)], GZ.at[at, xat(-1)], xr)
                landed(b, GZ.at[at, xat(1)], xl)
                if not 0 <= offset < 4:
                    send(e, GZ.at[at, xat(1)], GZ.at[at, xat(1)], xl)
                last.append((e, GZ.at[at, xat(2)], xr))
            forwards.clear()

        spread(0)
        yield
        for w in xs:
            landed(*w)
        mr, ml = [sem() for _ in range(4)], [sem() for _ in range(4)]
        send(mr[0], GX.at[z], GX.at[z], zr)
        send(ml[0], GX.at[z], GX.at[z], zl)
        for k in (1, 2, 3, 4):
            back, front = zat(-k), zat(k)
            if k < 4:
                landed(nr[k - 1], GZ.at[back, x], zr)
                rows = (GZ.at[back, x], GZ.at[back, x, low, :])[k == 3]
                send(nr[k], rows, rows, zr)
                landed(nl[k - 1], GZ.at[front, x], zl)
                rows = (GZ.at[front, x], GZ.at[front, x, high, :])[k == 3]
                send(nl[k], rows, rows, zl)
                pending = list(forwards)
                spread(-k)
                spread(k)
                added = forwards[len(pending) :]
                forwards[:] = pending
                forward()
                forwards[:] = added
                landed(mr[k - 1], GX.at[back], zr)
                rows = (GX.at[back], GX.at[back, lowx])[k == 3]
                send(mr[k], rows, rows, zr)
                landed(ml[k - 1], GX.at[front], zl)
                rows = (GX.at[front], GX.at[front, highx])[k == 3]
                send(ml[k], rows, rows, zl)
            else:
                landed(nr[3], GZ.at[back, x, low, :], zr)
                landed(nl[3], GZ.at[back, x, high, :], zl)
                spread(4)
                forward()
                landed(mr[3], GX.at[back, lowx], zr)
                landed(ml[3], GX.at[back, highx], zl)
            yield
        for w in last:
            landed(*w)
        yield

    one = plane(GX1, GZ1, y1)
    tokens = token_steps()
    next(one)
    y2 = over_y(((GX2, ix2), (GZ2, iz2)))

    ns = [sem() for _ in range(3)]

    @pl.when(f == x)
    def _():
        ST[...] = start[f]
        for i, k in enumerate((1, 2, 3)):
            copy(ns[i], start.at[fat(k)], ST, {"fs": fat(k)}).start()

    next(one)
    next(tokens)
    next(one)
    two = plane(GX2, GZ2, y2)
    next(two)
    next(one)
    next(tokens)
    next(one)
    next(tokens)
    next(one)
    for w in relay_waits + shift_waits:
        landed(*w)

    i0 = lax.broadcasted_iota(jnp.int32, (BLOCK, BLOCK), 0)
    i1 = lax.broadcasted_iota(jnp.int32, (BLOCK, BLOCK), 1)
    causal = i0 >= i1
    tril = jnp.where(causal, 1.0, 0.0).astype(BF16)
    my_room = room[pl.ds(f, 1), :]

    def project(s, _):
        x0, x1 = T[0, s], T[1, s]
        half = NZ // 2
        pa = dot(x0, GX1[:half].reshape(1024, WX1)) + dot(x1, GX1[half:].reshape(1024, WX1))
        pb = dot(x0, GZ1[:half].reshape(1024, WZ1)) + dot(x1, GZ1[half:].reshape(1024, WZ1))
        w0, w1 = x0.astype(F32), x1.astype(F32)
        square = jnp.sum(w0 * w0 + w1 * w1, axis=1, keepdims=True)
        scale = lax.rsqrt(square * (1.0 / 2048) + EPSILON)
        pa, pb = pa * scale, pb * scale
        keys = my_room * jax.nn.sigmoid(-pa[:, :128])
        query = pa[:, 128:]
        Q[s] = query * jax.nn.sigmoid(query) * HEAD ** (-0.5)
        K[s] = keys
        value = pb[:, :128].astype(BF16)
        V[s] = value
        gate = pb[:, 128:256]
        G[s] = gate * jax.nn.sigmoid(gate) * hgain[...]
        pool = pb[:, 256:].astype(BF16)
        EXT[s, 128:384, :] = pool
        BS[s] = pool[240:256]
        lag = SH[s, pl.ds(f, 1), :]
        ends, adds = [], []
        for b in range(2):
            rows = slice(b * BLOCK, (b + 1) * BLOCK)
            lags = jnp.transpose(jnp.broadcast_to(lag[:, rows], (BLOCK, BLOCK)))
            decay = jnp.log1p(-keys[rows]) + lags
            high = decay.astype(BF16)
            rest = decay - high.astype(F32)
            mid = rest.astype(BF16)
            low = (rest - mid.astype(F32)).astype(BF16)
            within = dot(tril, high) + dot(tril, mid) + dot(tril, low)
            C[s, rows, :] = within
            end = within[BLOCK - 1 :]
            adds.append(dot(value[rows], (keys[rows] * jnp.exp(end - within)).astype(BF16), TN))
            ends.append(end)
        A0[s] = adds[0]
        SL[s] = pack_state(jnp.exp(ends[1]) * adds[0] + adds[1], ends[0] + ends[1])
        return 0

    lax.fori_loop(0, 4, project, 0)

    sx = []
    SR[x] = SL[x]
    for k in (1, 3, 2):
        n = sem()
        send(n, SL.at[xat(k)], SR.at[x], {"sp_1": xat(k)})
        sx.append((n, SR.at[xat(-k)], {"sp_1": xat(k)}))
    nb = sem()
    send(nb, BS, BR, nxt)
    next(two)

    for w in sx:
        landed(*w)
    state, decay = unpack_state(SR[0])
    for i in range(1, NX):
        later, fade = unpack_state(SR[i])
        state, decay = jnp.exp(fade) * state + later, decay + fade
    ZS[...] = pack_state(state, decay)
    sz = []
    for k in (4, 3, 5, 2, 6, 1, 7):
        n = sem()
        send(n, ZS, ZR.at[z], {"sp_0": zat(k)})
        sz.append((n, ZR.at[zat(-k)], {"sp_0": zat(k)}))

    def inner(s, _):
        for b in range(2):
            rows = slice(b * BLOCK, (b + 1) * BLOCK)
            within = C[s, rows, :]
            centre = within[BLOCK // 2 - 1 : BLOCK // 2]
            query, keys = Q[s, rows, :], K[s, rows, :]
            scores = dot(
                (query * jnp.exp(within - centre)).astype(BF16),
                (keys * jnp.exp(centre - within)).astype(BF16),
                NT,
            )
            scores = jnp.where(causal, scores, 0.0).astype(BF16)
            INS[s, rows, :] = dot(scores, V[s, rows, :])
            QE[s, rows, :] = (query * jnp.exp(within)).astype(BF16)
        return 0

    lax.fori_loop(0, 4, inner, 0)
    next(two)

    landed(nb, BR, nxt)
    span = lax.shift_left(jnp.int32(2), c * 2 + f // 2)
    ti = lax.broadcasted_iota(jnp.int32, (256, 384), 0)
    si = lax.broadcasted_iota(jnp.int32, (256, 384), 1) - 128
    band = jnp.where((si <= ti) & (si > ti - span) & (si >= -16), 1.0, 0.0).astype(BF16)
    position = here * 256 + lax.broadcasted_iota(jnp.int32, (256, 128), 0)
    amount = jnp.minimum(position + 1, span).astype(F32)

    def pool(s, _):
        EXT[s, 0:128, :] = jnp.zeros((128, 128), BF16)

        @pl.when(here > 0)
        def _():
            EXT[s, 112:128, :] = BR[s]

        window = dot(band, EXT[s])
        PO[s] = (window / amount - EXT[s, 128:384, :].astype(F32)).astype(BF16)
        return 0

    lax.fori_loop(0, 4, pool, 0)
    act_waits = []

    def give_back(buffer, slot):
        ACT[slot + f] = buffer[f]
        for k in (1, 3, 2):
            n = sem()
            send(n, buffer.at[fat(k)], ACT.at[slot + f], {"fs": fat(k)})
            act_waits.append((n, ACT.at[slot + fat(-k)], {"fs": fat(k)}))

    give_back(PO, 4)

    for w in sz:
        landed(*w)
    for i, k in enumerate((1, 2, 3)):

        @pl.when(fat(-k) == x)
        def _(i=i, k=k):
            landed(ns[i], ST, {"fs": fat(k)})

    def pass_z(i, state):
        later, fade = unpack_state(ZR[i])
        return jnp.exp(fade) * state + later

    state = lax.fori_loop(0, z, pass_z, ST[...].astype(F32))
    for i in range(NX):
        ES[i] = state.astype(BF16)
        if i < NX - 1:
            later, fade = unpack_state(SR[i])
            state = jnp.exp(fade) * state + later
    sb = []
    ER[x] = ES[x]
    for k in (1, 3, 2):
        n = sem()
        send(n, ES.at[xat(k)], ER.at[x], {"sp_1": xat(k)})
        sb.append((n, ER.at[xat(-k)], {"sp_1": xat(k)}))
    next(two)
    for w in sb:
        landed(*w)

    def finish(s, _):
        entering = ER[s].astype(F32)
        middle = jnp.exp(C[s, BLOCK - 1 : BLOCK, :]) * entering + A0[s]
        for b, state in enumerate((ER[s], middle.astype(BF16))):
            rows = slice(b * BLOCK, (b + 1) * BLOCK)
            raw = INS[s, rows, :] + dot(QE[s, rows, :], state, NT)
            square = jnp.mean(raw * raw, axis=1, keepdims=True)
            RO[s, rows, :] = (raw * lax.rsqrt(square + EPSILON) * G[s, rows, :]).astype(BF16)
        return 0

    lax.fori_loop(0, 4, finish, 0)
    give_back(RO, 0)
    next(two)
    next(two)
    for w in act_waits:
        landed(*w)

    def rows_of(core):
        rows = pl.ds(pl.multiple_of(core * 128, 128), 128)
        parts = [ACT[i, rows, :] for i in range(8)]
        return jnp.concatenate(parts[:3], axis=1), jnp.concatenate(parts[3:], axis=1)

    ax, az = rows_of(other)
    for i in range(4):
        wx = GX2[2 * i : 2 * i + 2].reshape(512, WX2)
        wz = GZ2[2 * i : 2 * i + 2].reshape(512, WZ2)
        PS[:, 512 * i : 512 * i + 512] = (dot(ax, wx, NT) + dot(az, wz, NT)).astype(BF16)
    n = sem()
    send(n, PS, PR, {"tp": other})
    ax, az = rows_of(c)
    own = []
    for i in range(4):
        wx = GX2[2 * i : 2 * i + 2].reshape(512, WX2)
        wz = GZ2[2 * i : 2 * i + 2].reshape(512, WZ2)
        own.append((dot(ax, wx, NT) + dot(az, wz, NT)).astype(BF16))
    landed(n, PR, {"tp": other})
    for i in range(4):
        cols = slice(512 * i, 512 * i + 512)
        out[:, cols] = (own[i].astype(F32) + PR[:, cols].astype(F32)).astype(BF16)

    for made in sent:
        made.wait_send()

    @pl.when(f == x)
    def _():
        for i, k in enumerate((1, 2, 3)):
            copy(ns[i], start.at[fat(k)], ST, {"fs": fat(k)}).wait_send()


def per_device(
    tokens,
    norm_gain,
    query_weight,
    forget_weight,
    value_weight,
    outgate_weight,
    pool_in_weight,
    forget_room,
    decay_shift,
    head_gain,
    start_state,
    pool_map,
    pool_scale,
    out_rec_weight,
    out_pool_weight,
):
    row = lax.axis_index(SP_FS) * 16
    gain = lax.dynamic_slice(norm_gain, (row,), (16,))[:, None]

    def split(w):
        return w.reshape(16, 4, 128).transpose(1, 0, 2)

    def scaled(w):
        return split((w.astype(F32) * gain).astype(BF16))

    folded = jnp.einsum(
        "rgc,gcd->rgd",
        pool_in_weight.reshape(16, 2, POOL_DIM),
        pool_map,
        preferred_element_type=F32,
    ).reshape(16, 512)
    pool = split((folded * gain * pool_scale[None, :]).astype(BF16))
    out_t = jnp.concatenate([out_rec_weight, out_pool_weight], axis=0).T
    out_all = jnp.broadcast_to(out_t[None], (4, 16, 1024))
    ix1 = jnp.concatenate([scaled(forget_weight), scaled(query_weight)], axis=2)
    iz1 = jnp.concatenate([scaled(value_weight), scaled(outgate_weight), pool], axis=2)
    ix2, iz2 = out_all[:, :, :WX2], out_all[:, :, WX2:]
    shift = jnp.pad(decay_shift[0].T, ((0, 4), (0, 0)))
    start = start_state[0].transpose(0, 2, 1).astype(BF16)

    vmem = lambda *shape: pltpu.VMEM(shape, F32)
    half = lambda *shape: pltpu.VMEM(shape, BF16)
    mixed = pl.pallas_call(
        kernel,
        out_shape=jax.ShapeDtypeStruct((128, 2048), BF16),
        in_specs=[pl.BlockSpec(memory_space=pltpu.VMEM)] * 9,
        out_specs=pl.BlockSpec(memory_space=pltpu.VMEM),
        scratch_shapes=[
            half(2, 4, 256, 1024),
            half(NZ, NX, 64, WX1),
            half(NZ, NX, 64, WZ1),
            half(NZ, NX, 64, WX2),
            half(NZ, NX, 64, WZ2),
            vmem(4, 8, 256),
            half(128, 128),
            vmem(4, 256, 128),
            half(4, 256, 128),
            vmem(4, 256, 128),
            vmem(4, 256, 128),
            vmem(4, 256, 128),
            half(4, 256, 128),
            vmem(4, 256, 128),
            vmem(4, 128, 128),
            half(4, 144, 128),
            half(4, 144, 128),
            half(144, 128),
            half(NZ, 144, 128),
            half(4, 128, 128),
            half(4, 128, 128),
            half(4, 384, 128),
            half(4, 16, 128),
            half(4, 16, 128),
            half(4, 256, 128),
            half(4, 256, 128),
            half(8, 256, 128),
            half(128, 2048),
            half(128, 2048),
            pltpu.SemaphoreType.DMA((NSEM,)),
            pltpu.SemaphoreType.DMA((NSEM,)),
        ],
        compiler_params=pltpu.CompilerParams(
            collective_id=0, has_side_effects=True, vmem_limit_bytes=60 * 1024 * 1024
        ),
    )(
        tokens[0],
        ix1,
        iz1,
        ix2,
        iz2,
        forget_room.reshape(4, 128),
        shift,
        head_gain.reshape(1, 128),
        start,
    )
    return mixed[None]


def solution(mesh):
    finer = Mesh(
        mesh.devices.reshape(8, 4, mesh.shape["fs"], mesh.shape["tp"]), ("sp_0", "sp_1", "fs", "tp")
    )
    placed = (
        P("fs", SP, "tp"),
        P(),
        P(SP_FS, "tp"),
        P(SP_FS, "tp"),
        P(SP_FS, "tp"),
        P(SP_FS, "tp"),
        P(SP_FS, "tp"),
        P("tp"),
        P("fs", SP, "tp"),
        P(),
        P("fs", "tp", None, None),
        P("tp", None, None),
        P("tp"),
        P("tp", SP_FS),
        P("tp", SP_FS),
    )
    return jax.shard_map(
        per_device, mesh=finer, in_specs=placed, out_specs=P("fs", SP_TP, None), check_vma=False
    )
```

time: 266 us -> 98.6 us (0.37)
  waiting for transfers between devices: 161 us -> 0 us
  Pallas kernels: 0 us -> 89.3 us
  blocking collectives: 38.6 us -> 0 us
  matrix products: 20 us -> 0.15 us
  between operations: 14 us -> 0.13 us
  other arithmetic: 14.4 us -> 1.41 us
  starting transfers between devices: 8.06 us -> 0 us
    all_gather x2 -> x0, waiting for transfers between devices: 161 us -> none  [the longest x1 132 us: gather_turned(): filled, at, done = (lax.all_gather(both, axis, axis=0, tiled=True), 0, [])]
    pallas_call x0 -> x1, Pallas kernels: none -> 89.3 us  [per_device(): pl.pallas_call(kernel, out_shape=jax.ShapeDtypeStruct((128, 2048), BF16),...]
    all_gather x3 -> x0, blocking collectives: 28.7 us -> none  [entering_2(): lax.all_gather(part.astype(kind), axis)]
    dot_general x10 -> x1, matrix products: 20 us -> 0.15 us  [per_device(): jnp.einsum('rgc,gcd->rgd', pool_in_weight.reshape(16, 2, POOL_DIM), pool_...]
    all_to_all x1 -> x0, blocking collectives: 9.93 us -> none  [sum_at_owner(): lax.all_to_all(blocks, axis, split_axis=0, concat_axis=0, tiled=True)]
    all_to_all x1 -> x0, starting transfers between devices: 6.77 us -> none  [from_everyone(): lax.all_to_all(jnp.broadcast_to(array[None], (count, *array.shape)), axis...]
    convert_element_type x16 -> x0, other arithmetic: 6.23 us -> none  [the longest x8 3.62 us: per_device(): window_sum = window_sum + extended[WIDEST - offset:WIDEST - offset + leng...]
  transfers between devices with their start and end apart: 4 -> 0, of which waited for: 2 -> 0; matrix products, arithmetic and copies ran while one was open for 6% -> 0% of each run, Pallas kernels for 0% -> 0%
where the time goes in v1:
time: 98.6 us; the launch traced here: 97.8 us
  Pallas kernels  89.3 us (91%)
  local copies, waits for them, and re-layouts  6.84 us (7%)
  other arithmetic  1.41 us (1%)
    pallas_call x1, Pallas kernels, per_device(): pl.pallas_call(kernel, out_shape=jax.ShapeDtypeStruct((128, 2048), BF16),...  89.3 us
    unnamed x26, local copies, waits for them, and re-layouts  4.03 us

profile of v1, /device:TPU:1, one launch (start us, length us, event | category | flops | bytes accessed | tf_op | source)
XLA Modules:
  0.0 97.8 jit_solution(15980601042258372232)
XLA Ops:
  0.0 0.0 copy-start
  0.0 0.0 copy-start.10
  0.0 0.0 copy-start.5
  0.0 0.0 copy-start.4
  0.0 0.8 dynamic_slice.3
  0.8 0.0 copy-done.10
  0.8 0.6 pad.4.shift
  1.4 0.0 copy-done.5
  1.4 0.0 copy-done.4
  1.4 0.0 copy-start.2
  1.5 0.0 copy-start.3
  1.5 0.6 copy-done.2
  2.1 0.0 copy-done
  2.1 0.1 copy-done.3
  2.2 0.1 convolution_bitcast_fusion
  2.4 0.0 copy-start.11
  2.4 0.6 copy-done.11
  3.1 0.1 fusion.6
  3.1 0.0 slice-start
  3.1 0.0 copy-start.6
  3.1 0.0 copy-start.7
  3.2 0.0 copy-start.8
  3.2 0.0 copy-start.9
  3.2 0.6 broadcast_in_dim.6.ix2
  3.8 0.1 slice-done
  3.9 0.0 copy-start.1
  3.9 0.6 broadcast_in_dim.14.iz2
  4.5 0.0 copy-done.6
  4.5 0.0 copy-done.7
  4.5 0.0 copy-done.8
  4.5 0.0 copy-done.9
  4.5 0.1 fusion.4
  4.6 0.6 pad_maximum_fusion.iz1
  5.3 0.6 pad_maximum_fusion.1.ix1
  5.9 0.0 copy-done.1
  5.9 0.8 copy.25
  6.6 89.3 %shard_map.145 = bf16[128,2048]{1,0:T(8,128)(2,1)} custom-call(bf16[256,1024]{1,0:T(8,128)(2,1)} %bitcast.50, bf16[4,16,256]{2,1,0:T(8,128)(2,1)} %pad_maximum_fusion.1.ix1, bf16[4,16,384]{2,1,0:T(8,128)(2,1)} %pad_maximum_fusion.iz1, bf16[4,16,384]{2,1,0:T(8,128)(2,1)} %broadcast_in_dim.6.ix2, bf16[4,16,640]{2,1,0:T(8,128)(2,1)} %broadcast_in_dim.14.iz2, ...), custom_call_target="tpu_custom_call" | custom-call | tf_op jit(solution)/shard_map/pallas_call | solution.py:540
  95.9 1.9 %copy.47 = bf16[1,128,2048]{2,1,0:T(8,128)(2,1)} copy(bf16[1,128,2048]{2,1,0:T(8,128)(2,1)} %bitcast.48) | data formatting | bytes 1048576
  (6 shorter events, 0.1 us)
Async XLA Ops:
  0.0 2.1 %copy-start = (bf16[2,256,256]{2,1,0:T(8,128)(2,1)S(1)}, bf16[2,256,256]{2,1,0:T(8,128)(2,1)}, u32[]{:S(2)}) copy-start(bf16[2,256,256]{2,1,0:T(8,128)(2,1)} %param.26) | copy-start | bytes 786436
  0.0 0.8 copy-start.10
  0.0 1.4 %copy-start.5 = (bf16[512,16]{0,1:T(8,128)(2,1)S(1)}, bf16[512,16]{0,1:T(8,128)(2,1)}, u32[]{:S(2)}) copy-start(bf16[512,16]{0,1:T(8,128)(2,1)} %param.28) | copy-start | bytes 49156
  0.0 1.4 %copy-start.4 = (bf16[512,16]{0,1:T(8,128)(2,1)S(1)}, bf16[512,16]{0,1:T(8,128)(2,1)}, u32[]{:S(2)}) copy-start(bf16[512,16]{0,1:T(8,128)(2,1)} %param.29) | copy-start | bytes 49156
  1.4 0.6 copy-start.2
  1.5 0.7 copy-start.3
  2.4 0.7 copy-start.11
  3.1 0.7 slice-start
  3.1 1.4 %copy-start.6 = (bf16[16,512]{1,0:T(8,128)(2,1)S(1)}, bf16[16,512]{1,0:T(8,128)(2,1)}, u32[]{:S(2)}) copy-start(bf16[16,512]{1,0:T(8,128)(2,1)} %param.19) | copy-start | bytes 49156
  3.1 1.4 %copy-start.7 = (bf16[16,512]{1,0:T(8,128)(2,1)S(1)}, bf16[16,512]{1,0:T(8,128)(2,1)}, u32[]{:S(2)}) copy-start(bf16[16,512]{1,0:T(8,128)(2,1)} %param.17) | copy-start | bytes 49156
  3.2 1.4 %copy-start.8 = (bf16[16,512]{1,0:T(8,128)(2,1)S(1)}, bf16[16,512]{1,0:T(8,128)(2,1)}, u32[]{:S(2)}) copy-start(bf16[16,512]{1,0:T(8,128)(2,1)} %param.20) | copy-start | bytes 49156
  3.2 1.3 %copy-start.9 = (bf16[16,512]{1,0:T(8,128)(2,1)S(1)}, bf16[16,512]{1,0:T(8,128)(2,1)}, u32[]{:S(2)}) copy-start(bf16[16,512]{1,0:T(8,128)(2,1)} %param.18) | copy-start | bytes 49156
  3.9 2.0 %copy-start.1 = (f32[1,4,128,128]{3,2,1,0:T(8,128)S(1)}, f32[1,4,128,128]{3,2,1,0:T(8,128)}, u32[]{:S(2)}) copy-start(f32[1,4,128,128]{3,2,1,0:T(8,128)} %param.25) | copy-start | bytes 786436

commit v2 on v1

--- a/solution.py
+++ b/solution.py
@@ -14,9 +14,9 @@
 SP_TP = ("sp_0", "sp_1", "tp")
 EPSILON = 1e-06
 MESH = pl.DeviceIdType.MESH
-NSEM = 160
+NSEM = 288
 NZ, NX, NF = 8, 4, 4
-WX1, WZ1, WX2, WZ2 = 256, 384, 384, 640
+WX, WZ, WB, WBX = (256, 256), (256, 128, 384), 384, 128
 F32, BF16 = jnp.float32, jnp.bfloat16
 NT = (((1,), (1,)), ((), ()))
 TN = (((0,), (0,)), ((), ()))
@@ -27,13 +27,17 @@
 
 
 def pack_state(state, decay):
-    high = decay.astype(BF16).astype(F32)
-    rest = decay - high
-    mid = rest.astype(BF16).astype(F32)
-    low = rest - mid
+    high, mid, low = three_parts(decay)
     row = lax.broadcasted_iota(jnp.int32, (16, HEAD), 0)
     tail = jnp.where(row == 0, high, jnp.where(row == 1, mid, jnp.where(row == 2, low, 0.0)))
     return jnp.concatenate([state, tail], axis=0).astype(BF16)
+
+
+def three_parts(value):
+    high = value.astype(BF16).astype(F32)
+    rest = value - high
+    mid = rest.astype(BF16).astype(F32)
+    return high, mid, rest - mid
 
 
 def unpack_state(packed):
@@ -44,20 +48,24 @@
 
 def kernel(
     tok,
-    ix1,
     iz1,
     ix2,
     iz2,
+    ix3,
+    iz3,
+    ib,
     room,
     shift,
     hgain,
     start,
     out,
     T,
-    GX1,
     GZ1,
     GX2,
     GZ2,
+    GX3,
+    GZ3,
+    GB,
     SH,
     ST,
     K,
@@ -82,6 +90,7 @@
     ACT,
     PS,
     PR,
+    SC,
     send_sems,
     recv_sems,
 ):
@@ -131,8 +140,10 @@
         copy(n, dst, dst, who).wait_recv()
 
     mine = pl.ds(pl.multiple_of(f * 16, 16), 16)
-    for buffer, own in ((GX1, ix1), (GZ1, iz1), (GX2, ix2), (GZ2, iz2)):
+    pieces = ((GZ1, iz1), (GX2, ix2), (GZ2, iz2), (GX3, ix3), (GZ3, iz3))
+    for buffer, own in pieces:
         buffer[z, x, mine, :] = own[f]
+    GB[z, x, mine, :] = ib[...]
     T[c, f] = tok[...]
     SH[f] = shift[...]
 
@@ -149,7 +160,9 @@
                 waits.append((n, buffer.at[z, x, theirs, :], {"fs": to}))
         return waits
 
-    y1 = over_y(((GX1, ix1), (GZ1, iz1)))
+    y1 = over_y(pieces[:1])
+    y2 = over_y(pieces[1:3])
+    y3 = over_y(pieces[3:])
     shift_waits = []
     for k in (1, 3, 2):
         n = sem()
@@ -193,88 +206,126 @@
         relay(fat(2), second)
         yield
 
-    def plane(GX, GZ, waits):
+    def plane(waits, vx, vz):
         zr, zl = {"sp_0": zat(1)}, {"sp_0": zat(-1)}
         xr, xl = {"sp_1": xat(1)}, {"sp_1": xat(-1)}
-        low, high = pl.ds(0, 32), pl.ds(32, 32)
-        lowx, highx = pl.ds(0, 2), pl.ds(2, 2)
+        whole, lowx, highx = pl.ds(0, 4), pl.ds(0, 2), pl.ds(2, 2)
         for w in waits:
             landed(*w)
         xs = []
-        for k in (1, 3, 2):
+        for k in (1, 3, 2) if vx else ():
             n = sem()
-            send(n, GX.at[z, x], GX.at[z, x], {"sp_1": xat(k)})
-            xs.append((n, GX.at[z, xat(-k)], {"sp_1": xat(k)}))
+            send(n, vx(z, x), vx(z, x), {"sp_1": xat(k)})
+            xs.append((n, vx(z, xat(-k)), {"sp_1": xat(k)}))
         nr, nl = [sem() for _ in range(4)], [sem() for _ in range(4)]
-        send(nr[0], GZ.at[z, x], GZ.at[z, x], zr)
-        send(nl[0], GZ.at[z, x], GZ.at[z, x], zl)
+        send(nr[0], vz(z, x), vz(z, x), zr)
+        send(nl[0], vz(z, x), vz(z, x), zl)
         forwards = []
         last = []
 
         def spread(offset):
             at = zat(offset)
             a, b, e = sem(), sem(), sem()
-            send(a, GZ.at[at, x], GZ.at[at, x], xr)
-            send(b, GZ.at[at, x], GZ.at[at, x], xl)
+            send(a, vz(at, x), vz(at, x), xr)
+            send(b, vz(at, x), vz(at, x), xl)
             forwards.append((offset, a, b, e))
 
-        def forward():
-            for offset, a, b, e in forwards:
+        def forward(ready):
+            for offset, a, b, e in ready:
                 at = zat(offset)
-                landed(a, GZ.at[at, xat(-1)], xr)
+                landed(a, vz(at, xat(-1)), xr)
                 if 0 <= offset < 4:
-                    send(e, GZ.at[at, xat(-1)], GZ.at[at, xat(-1)], xr)
-                landed(b, GZ.at[at, xat(1)], xl)
+                    send(e, vz(at, xat(-1)), vz(at, xat(-1)), xr)
+                landed(b, vz(at, xat(1)), xl)
                 if not 0 <= offset < 4:
-                    send(e, GZ.at[at, xat(1)], GZ.at[at, xat(1)], xl)
-                last.append((e, GZ.at[at, xat(2)], xr))
+                    send(e, vz(at, xat(1)), vz(at, xat(1)), xl)
+                last.append((e, vz(at, xat(2)), xr))
+
+        spread(0)
+        yield
+        if vx:
+            for w in xs:
+                landed(*w)
+            mr, ml = [sem() for _ in range(4)], [sem() for _ in range(4)]
+            send(mr[0], vx(z, whole), vx(z, whole), zr)
+            send(ml[0], vx(z, whole), vx(z, whole), zl)
+            yield
+        for k in (1, 2, 3):
+            back, front = zat(-k), zat(k)
+            landed(nr[k - 1], vz(back, x), zr)
+            part = vz(back, x, 1 if k == 3 else 0)
+            send(nr[k], part, part, zr)
+            landed(nl[k - 1], vz(front, x), zl)
+            part = vz(front, x, 2 if k == 3 else 0)
+            send(nl[k], part, part, zl)
+            ready = list(forwards)
             forwards.clear()
-
-        spread(0)
-        yield
-        for w in xs:
-            landed(*w)
-        mr, ml = [sem() for _ in range(4)], [sem() for _ in range(4)]
-        send(mr[0], GX.at[z], GX.at[z], zr)
-        send(ml[0], GX.at[z], GX.at[z], zl)
-        for k in (1, 2, 3, 4):
-            back, front = zat(-k), zat(k)
-            if k < 4:
-                landed(nr[k - 1], GZ.at[back, x], zr)
-                rows = (GZ.at[back, x], GZ.at[back, x, low, :])[k == 3]
-                send(nr[k], rows, rows, zr)
-                landed(nl[k - 1], GZ.at[front, x], zl)
-                rows = (GZ.at[front, x], GZ.at[front, x, high, :])[k == 3]
-                send(nl[k], rows, rows, zl)
-                pending = list(forwards)
-                spread(-k)
-                spread(k)
-                added = forwards[len(pending) :]
-                forwards[:] = pending
-                forward()
-                forwards[:] = added
-                landed(mr[k - 1], GX.at[back], zr)
-                rows = (GX.at[back], GX.at[back, lowx])[k == 3]
-                send(mr[k], rows, rows, zr)
-                landed(ml[k - 1], GX.at[front], zl)
-                rows = (GX.at[front], GX.at[front, highx])[k == 3]
-                send(ml[k], rows, rows, zl)
-            else:
-                landed(nr[3], GZ.at[back, x, low, :], zr)
-                landed(nl[3], GZ.at[back, x, high, :], zl)
-                spread(4)
-                forward()
-                landed(mr[3], GX.at[back, lowx], zr)
-                landed(ml[3], GX.at[back, highx], zl)
+            spread(-k)
+            spread(k)
+            if vx:
+                landed(mr[k - 1], vx(back, whole), zr)
+                part = vx(back, lowx if k == 3 else whole)
+                send(mr[k], part, part, zr)
+                landed(ml[k - 1], vx(front, whole), zl)
+                part = vx(front, highx if k == 3 else whole)
+                send(ml[k], part, part, zl)
+            forward(ready)
             yield
+        far = zat(4)
+        landed(nr[3], vz(far, x, 1), zr)
+        landed(nl[3], vz(far, x, 2), zl)
+        spread(4)
+        forward(forwards)
+        if vx:
+            landed(mr[3], vx(far, lowx), zr)
+            landed(ml[3], vx(far, highx), zl)
+        yield
         for w in last:
             landed(*w)
         yield
 
-    one = plane(GX1, GZ1, y1)
+    def views(GX, GZ):
+        halves = (None, pl.ds(0, 32), pl.ds(32, 32))
+
+        def vz(zi, xi, part=0):
+            return GZ.at[zi, xi, halves[part], :] if part else GZ.at[zi, xi]
+
+        return (GX is not None) and (lambda zi, xi: GX.at[zi, xi]), vz
+
+    lanes = (pl.ds(WBX, WB - WBX), pl.ds(WBX, 128), pl.ds(WBX + 128, 128))
+    late = plane(
+        (),
+        lambda zi, xi: GB.at[zi, xi, mine, pl.ds(0, WBX)],
+        lambda zi, xi, part=0: GB.at[zi, xi, mine, lanes[part]],
+    )
+
+    def late_over_y():
+        first, second = pl.ds(0, 4), pl.ds(4, 4)
+
+        def part(k, half):
+            rows = pl.ds(pl.multiple_of(fat(k) * 16, 16), 16)
+            return GB.at[half, :, rows, :]
+
+        br, bl = [sem() for _ in range(3)], [sem() for _ in range(3)]
+        for i, (a, b) in enumerate(((first, second), (second, first))):
+            send(br[i], part(0, a), part(0, a), right)
+            send(bl[i], part(0, b), part(0, b), left)
+        yield
+        landed(br[0], part(-1, first), right)
+        send(br[2], part(-1, first), part(-1, first), right)
+        landed(bl[0], part(1, second), left)
+        send(bl[2], part(1, second), part(1, second), left)
+        yield
+        landed(br[1], part(-1, second), right)
+        landed(bl[1], part(1, first), left)
+        landed(br[2], part(-2, first), right)
+        landed(bl[2], part(2, second), left)
+        yield
+
+    one = plane(y1, *views(None, GZ1))
+    two = plane(y2, *views(GX2, GZ2))
+    three = plane(y3, *views(GX3, GZ3))
     tokens = token_steps()
-    next(one)
-    y2 = over_y(((GX2, ix2), (GZ2, iz2)))
 
     ns = [sem() for _ in range(3)]
 
@@ -284,56 +335,64 @@
         for i, k in enumerate((1, 2, 3)):
             copy(ns[i], start.at[fat(k)], ST, {"fs": fat(k)}).start()
 
+    next(late)
+    next(one)
+    next(two)
+    next(late)
     next(one)
     next(tokens)
     next(one)
-    two = plane(GX2, GZ2, y2)
     next(two)
+    next(late)
     next(one)
     next(tokens)
     next(one)
-    next(tokens)
+    next(late)
+    next(two)
+    next(three)
     next(one)
     for w in relay_waits + shift_waits:
         landed(*w)
+    relay_waits.clear()
 
     i0 = lax.broadcasted_iota(jnp.int32, (BLOCK, BLOCK), 0)
     i1 = lax.broadcasted_iota(jnp.int32, (BLOCK, BLOCK), 1)
     causal = i0 >= i1
     tril = jnp.where(causal, 1.0, 0.0).astype(BF16)
+    ones = jnp.ones((BLOCK, BLOCK), BF16)
     my_room = room[pl.ds(f, 1), :]
 
+    half = NZ // 2
+
+    def each(body):
+        for s in range(4):
+            body(s, 0)
+
+    def through(s, *weights):
+        low = jnp.concatenate([w[:half].reshape(1024, w.shape[-1]) for w in weights], axis=1)
+        high = jnp.concatenate([w[half:].reshape(1024, w.shape[-1]) for w in weights], axis=1)
+        return (dot(T[0, s], low) + dot(T[1, s], high)) * SC[s]
+
     def project(s, _):
-        x0, x1 = T[0, s], T[1, s]
-        half = NZ // 2
-        pa = dot(x0, GX1[:half].reshape(1024, WX1)) + dot(x1, GX1[half:].reshape(1024, WX1))
-        pb = dot(x0, GZ1[:half].reshape(1024, WZ1)) + dot(x1, GZ1[half:].reshape(1024, WZ1))
-        w0, w1 = x0.astype(F32), x1.astype(F32)
+        w0, w1 = T[0, s].astype(F32), T[1, s].astype(F32)
         square = jnp.sum(w0 * w0 + w1 * w1, axis=1, keepdims=True)
-        scale = lax.rsqrt(square * (1.0 / 2048) + EPSILON)
-        pa, pb = pa * scale, pb * scale
-        keys = my_room * jax.nn.sigmoid(-pa[:, :128])
-        query = pa[:, 128:]
-        Q[s] = query * jax.nn.sigmoid(query) * HEAD ** (-0.5)
+        SC[s] = lax.rsqrt(square * (1.0 / 2048) + EPSILON)
+        both = through(s, GZ1)
+        keys = my_room * jax.nn.sigmoid(-both[:, :128])
         K[s] = keys
-        value = pb[:, :128].astype(BF16)
+        value = both[:, 128:].astype(BF16)
         V[s] = value
-        gate = pb[:, 128:256]
-        G[s] = gate * jax.nn.sigmoid(gate) * hgain[...]
-        pool = pb[:, 256:].astype(BF16)
-        EXT[s, 128:384, :] = pool
-        BS[s] = pool[240:256]
         lag = SH[s, pl.ds(f, 1), :]
         ends, adds = [], []
         for b in range(2):
             rows = slice(b * BLOCK, (b + 1) * BLOCK)
-            lags = jnp.transpose(jnp.broadcast_to(lag[:, rows], (BLOCK, BLOCK)))
-            decay = jnp.log1p(-keys[rows]) + lags
-            high = decay.astype(BF16)
-            rest = decay - high.astype(F32)
-            mid = rest.astype(BF16)
-            low = (rest - mid.astype(F32)).astype(BF16)
-            within = dot(tril, high) + dot(tril, mid) + dot(tril, low)
+            lags = three_parts(lag[:, rows])
+            spread = [jnp.where(causal, jnp.broadcast_to(p, (BLOCK, BLOCK)), 0.0).astype(BF16) for p in lags]
+            parts = [p.astype(BF16) for p in three_parts(jnp.log1p(-keys[rows]))]
+            within = dot(
+                jnp.concatenate([tril] * 3 + spread, axis=1),
+                jnp.concatenate(parts + [ones] * 3, axis=0),
+            )
             C[s, rows, :] = within
             end = within[BLOCK - 1 :]
             adds.append(dot(value[rows], (keys[rows] * jnp.exp(end - within)).astype(BF16), TN))
@@ -342,7 +401,26 @@
         SL[s] = pack_state(jnp.exp(ends[1]) * adds[0] + adds[1], ends[0] + ends[1])
         return 0
 
-    lax.fori_loop(0, 4, project, 0)
+    for k in (0, -1, 1):
+        project(fat(k), 0)
+    next(two)
+    next(three)
+    next(late)
+    next(tokens)
+    for w in relay_waits:
+        landed(*w)
+    project(fat(2), 0)
+
+    def project_rest(s, _):
+        rest = through(s, GX2, GZ2)
+        query = rest[:, :128]
+        Q[s] = query * jax.nn.sigmoid(query) * HEAD ** (-0.5)
+        gate = rest[:, 128:256]
+        G[s] = gate * jax.nn.sigmoid(gate) * hgain[...]
+        pool = rest[:, 256:].astype(BF16)
+        EXT[s, 128:384, :] = pool
+        BS[s] = pool[240:256]
+        return 0
 
     sx = []
     SR[x] = SL[x]
@@ -350,10 +428,9 @@
         n = sem()
         send(n, SL.at[xat(k)], SR.at[x], {"sp_1": xat(k)})
         sx.append((n, SR.at[xat(-k)], {"sp_1": xat(k)}))
-    nb = sem()
-    send(nb, BS, BR, nxt)
     next(two)
-
+    next(late)
+    next(three)
     for w in sx:
         landed(*w)
     state, decay = unpack_state(SR[0])
@@ -366,6 +443,15 @@
         n = sem()
         send(n, ZS, ZR.at[z], {"sp_0": zat(k)})
         sz.append((n, ZR.at[zat(-k)], {"sp_0": zat(k)}))
+
+    next(two)
+    next(late)
+    late = late_over_y()
+    next(late)
+    next(two)
+    each(project_rest)
+    nb = sem()
+    send(nb, BS, BR, nxt)
 
     def inner(s, _):
         for b in range(2):
@@ -383,8 +469,9 @@
             QE[s, rows, :] = (query * jnp.exp(within)).astype(BF16)
         return 0
 
-    lax.fori_loop(0, 4, inner, 0)
-    next(two)
+    each(inner)
+    next(three)
+    next(late)
 
     landed(nb, BR, nxt)
     span = lax.shift_left(jnp.int32(2), c * 2 + f // 2)
@@ -405,7 +492,7 @@
         PO[s] = (window / amount - EXT[s, 128:384, :].astype(F32)).astype(BF16)
         return 0
 
-    lax.fori_loop(0, 4, pool, 0)
+    each(pool)
     act_waits = []
 
     def give_back(buffer, slot):
@@ -441,7 +528,7 @@
         n = sem()
         send(n, ES.at[xat(k)], ER.at[x], {"sp_1": xat(k)})
         sb.append((n, ER.at[xat(-k)], {"sp_1": xat(k)}))
-    next(two)
+    next(three)
     for w in sb:
         landed(*w)
 
@@ -455,35 +542,32 @@
             RO[s, rows, :] = (raw * lax.rsqrt(square + EPSILON) * G[s, rows, :]).astype(BF16)
         return 0
 
-    lax.fori_loop(0, 4, finish, 0)
+    each(finish)
     give_back(RO, 0)
-    next(two)
-    next(two)
+    next(three)
+    next(three)
+    next(late)
     for w in act_waits:
         landed(*w)
 
-    def rows_of(core):
-        rows = pl.ds(pl.multiple_of(core * 128, 128), 128)
-        parts = [ACT[i, rows, :] for i in range(8)]
-        return jnp.concatenate(parts[:3], axis=1), jnp.concatenate(parts[3:], axis=1)
-
-    ax, az = rows_of(other)
+    a, b, d = (
+        jnp.concatenate([ACT[i] for i in range(*span)], axis=1) for span in ((0, 2), (2, 5), (5, 8))
+    )
+    my_rows = pl.ds(pl.multiple_of(c * 128, 128), 128)
+    their_rows = pl.ds(pl.multiple_of(other * 128, 128), 128)
+    swaps = []
     for i in range(4):
-        wx = GX2[2 * i : 2 * i + 2].reshape(512, WX2)
-        wz = GZ2[2 * i : 2 * i + 2].reshape(512, WZ2)
-        PS[:, 512 * i : 512 * i + 512] = (dot(ax, wx, NT) + dot(az, wz, NT)).astype(BF16)
-    n = sem()
-    send(n, PS, PR, {"tp": other})
-    ax, az = rows_of(c)
-    own = []
-    for i in range(4):
-        wx = GX2[2 * i : 2 * i + 2].reshape(512, WX2)
-        wz = GZ2[2 * i : 2 * i + 2].reshape(512, WZ2)
-        own.append((dot(ax, wx, NT) + dot(az, wz, NT)).astype(BF16))
-    landed(n, PR, {"tp": other})
-    for i in range(4):
-        cols = slice(512 * i, 512 * i + 512)
-        out[:, cols] = (own[i].astype(F32) + PR[:, cols].astype(F32)).astype(BF16)
+        at, cols = slice(2 * i, 2 * i + 2), slice(512 * i, 512 * i + 512)
+        total = dot(a, GX3[at].reshape(512, 256), NT)
+        total += dot(b, GZ3[at].reshape(512, WZ[2]), NT)
+        total += dot(d, GB[at].reshape(512, WB), NT)
+        PS[:, cols] = total.astype(BF16)
+        n = sem()
+        send(n, PS.at[their_rows, pl.ds(512 * i, 512)], PR.at[:, pl.ds(512 * i, 512)], {"tp": other})
+        swaps.append((n, PR.at[:, pl.ds(512 * i, 512)], {"tp": other}))
+    for w in swaps:
+        landed(*w)
+    out[...] = (PS[my_rows, :].astype(F32) + PR[...].astype(F32)).astype(BF16)
 
     for made in sent:
         made.wait_send()
@@ -529,9 +613,10 @@
     pool = split((folded * gain * pool_scale[None, :]).astype(BF16))
     out_t = jnp.concatenate([out_rec_weight, out_pool_weight], axis=0).T
     out_all = jnp.broadcast_to(out_t[None], (4, 16, 1024))
-    ix1 = jnp.concatenate([scaled(forget_weight), scaled(query_weight)], axis=2)
-    iz1 = jnp.concatenate([scaled(value_weight), scaled(outgate_weight), pool], axis=2)
-    ix2, iz2 = out_all[:, :, :WX2], out_all[:, :, WX2:]
+    iz1 = jnp.concatenate([scaled(forget_weight), scaled(value_weight)], axis=2)
+    ix2 = jnp.concatenate([scaled(query_weight), scaled(outgate_weight)], axis=2)
+    iz2 = pool
+    ix3, iz3, ib = out_all[:, :, :256], out_all[:, :, 256:640], out_t[:, 640:]
     shift = jnp.pad(decay_shift[0].T, ((0, 4), (0, 0)))
     start = start_state[0].transpose(0, 2, 1).astype(BF16)
 
@@ -540,14 +625,16 @@
     mixed = pl.pallas_call(
         kernel,
         out_shape=jax.ShapeDtypeStruct((128, 2048), BF16),
-        in_specs=[pl.BlockSpec(memory_space=pltpu.VMEM)] * 9,
+        in_specs=[pl.BlockSpec(memory_space=pltpu.VMEM)] * 11,
         out_specs=pl.BlockSpec(memory_space=pltpu.VMEM),
         scratch_shapes=[
             half(2, 4, 256, 1024),
-            half(NZ, NX, 64, WX1),
-            half(NZ, NX, 64, WZ1),
-            half(NZ, NX, 64, WX2),
-            half(NZ, NX, 64, WZ2),
+            half(NZ, NX, 64, WZ[0]),
+            half(NZ, NX, 64, WX[0]),
+            half(NZ, NX, 64, WZ[1]),
+            half(NZ, NX, 64, WX[1]),
+            half(NZ, NX, 64, WZ[2]),
+            half(NZ, NX, 64, WB),
             vmem(4, 8, 256),
             half(128, 128),
             vmem(4, 256, 128),
@@ -570,8 +657,9 @@
             half(4, 256, 128),
             half(4, 256, 128),
             half(8, 256, 128),
+            half(256, 2048),
             half(128, 2048),
-            half(128, 2048),
+            vmem(4, 256, 1),
             pltpu.SemaphoreType.DMA((NSEM,)),
             pltpu.SemaphoreType.DMA((NSEM,)),
         ],
@@ -580,10 +668,12 @@
         ),
     )(
         tokens[0],
-        ix1,
         iz1,
         ix2,
         iz2,
+        ix3,
+        iz3,
+        ib,
         forget_room.reshape(4, 128),
         shift,
         head_gain.reshape(1, 128),

time: 98.6 us -> 93.9 us (0.952)
  Pallas kernels: 89.3 us -> 84.8 us
    pallas_call x1, Pallas kernels: 89.3 us -> 84.8 us  [per_device(): pl.pallas_call(kernel, out_shape=jax.ShapeDtypeStruct((128, 2048), BF16),...]
    unnamed x26 -> x24, local copies, waits for them, and re-layouts: 4.03 us -> 3.37 us
where the time goes in v2:
time: 93.9 us; the launch traced here: 93.7 us
  Pallas kernels  84.8 us (90%)
  local copies, waits for them, and re-layouts  6.67 us (7%)
  other arithmetic  1.97 us (2%)
    pallas_call x1, Pallas kernels, per_device(): pl.pallas_call(kernel, out_shape=jax.ShapeDtypeStruct((128, 2048), BF16),...  84.8 us
    unnamed x24, local copies, waits for them, and re-layouts  3.37 us

profile of v2, /device:TPU:1, one launch (start us, length us, event | category | flops | bytes accessed | tf_op | source)
XLA Modules:
  0.0 93.7 jit_solution(2205684382100592407)
XLA Ops:
  0.0 0.0 copy-start
  0.0 0.0 copy-start.9
  0.0 0.0 copy-start.4
  0.0 0.0 copy-start.3
  0.0 0.8 dynamic_slice.3
  0.8 0.0 copy-done.9
  0.8 0.6 pad.4.shift
  1.4 0.0 copy-done.4
  1.4 0.0 copy-done.3
  1.4 0.6 fusion.9
  2.0 0.0 copy-start.2
  2.1 0.6 broadcast_in_dim.6.ix3
  2.7 0.0 copy-done
  2.7 0.1 copy-done.2
  2.8 0.1 convolution_bitcast_fusion
  2.9 0.0 copy-start.10
  3.0 0.0 copy-start.5
  3.0 0.0 copy-start.6
  3.0 0.0 copy-start.7
  3.0 0.0 copy-start.8
  3.1 0.6 copy-done.10
  3.6 0.0 copy-start.1
  3.6 0.7 fusion.6.iz2
  4.3 0.6 broadcast_in_dim.14.iz3
  4.9 0.0 copy-done.5
  4.9 0.0 copy-done.6
  4.9 0.0 copy-done.7
  4.9 0.0 copy-done.8
  4.9 0.1 fusion.4
  5.0 0.6 pad_maximum_fusion.1.ix2
  5.6 0.6 pad_maximum_fusion.iz1
  6.2 0.0 copy-done.1
  6.2 0.8 copy.25
  7.0 84.8 %shard_map.145 = bf16[128,2048]{1,0:T(8,128)(2,1)} custom-call(bf16[256,1024]{1,0:T(8,128)(2,1)} %bitcast.50, bf16[4,16,256]{2,1,0:T(8,128)(2,1)} %pad_maximum_fusion.iz1, bf16[4,16,256]{2,1,0:T(8,128)(2,1)} %pad_maximum_fusion.1.ix2, bf16[4,16,128]{2,1,0:T(8,128)(2,1)} %fusion.6.iz2, bf16[4,16,256]{2,1,0:T(8,128)(2,1)} %broadcast_in_dim.6.ix3, ...), custom_call_target="tpu_custom_call" | custom-call | tf_op jit(solution)/shard_map/pallas_call | solution.py:625
  91.8 1.9 %copy.47 = bf16[1,128,2048]{2,1,0:T(8,128)(2,1)} copy(bf16[1,128,2048]{2,1,0:T(8,128)(2,1)} %bitcast.48) | data formatting | bytes 1048576
  (6 shorter events, 0.1 us)
Async XLA Ops:
  0.0 2.7 %copy-start = (bf16[2,256,256]{2,1,0:T(8,128)(2,1)S(1)}, bf16[2,256,256]{2,1,0:T(8,128)(2,1)}, u32[]{:S(2)}) copy-start(bf16[2,256,256]{2,1,0:T(8,128)(2,1)} %param.26) | copy-start | bytes 786436
  0.0 0.8 copy-start.9
  0.0 1.4 %copy-start.4 = (bf16[512,16]{0,1:T(8,128)(2,1)S(1)}, bf16[512,16]{0,1:T(8,128)(2,1)}, u32[]{:S(2)}) copy-start(bf16[512,16]{0,1:T(8,128)(2,1)} %param.28) | copy-start | bytes 49156
  0.0 1.4 %copy-start.3 = (bf16[512,16]{0,1:T(8,128)(2,1)S(1)}, bf16[512,16]{0,1:T(8,128)(2,1)}, u32[]{:S(2)}) copy-start(bf16[512,16]{0,1:T(8,128)(2,1)} %param.29) | copy-start | bytes 49156
  2.0 0.7 copy-start.2
  2.9 0.7 copy-start.10
  3.0 1.9 %copy-start.5 = (bf16[16,512]{1,0:T(8,128)(2,1)S(1)}, bf16[16,512]{1,0:T(8,128)(2,1)}, u32[]{:S(2)}) copy-start(bf16[16,512]{1,0:T(8,128)(2,1)} %param.17) | copy-start | bytes 49156
  3.0 1.9 %copy-start.6 = (bf16[16,512]{1,0:T(8,128)(2,1)S(1)}, bf16[16,512]{1,0:T(8,128)(2,1)}, u32[]{:S(2)}) copy-start(bf16[16,512]{1,0:T(8,128)(2,1)} %param.19) | copy-start | bytes 49156
  3.0 1.9 %copy-start.7 = (bf16[16,512]{1,0:T(8,128)(2,1)S(1)}, bf16[16,512]{1,0:T(8,128)(2,1)}, u32[]{:S(2)}) copy-start(bf16[16,512]{1,0:T(8,128)(2,1)} %param.20) | copy-start | bytes 49156
  3.0 1.9 %copy-start.8 = (bf16[16,512]{1,0:T(8,128)(2,1)S(1)}, bf16[16,512]{1,0:T(8,128)(2,1)}, u32[]{:S(2)}) copy-start(bf16[16,512]{1,0:T(8,128)(2,1)} %param.18) | copy-start | bytes 49156
  3.6 2.6 %copy-start.1 = (f32[1,4,128,128]{3,2,1,0:T(8,128)S(1)}, f32[1,4,128,128]{3,2,1,0:T(8,128)}, u32[]{:S(2)}) copy-start(f32[1,4,128,128]{3,2,1,0:T(8,128)} %param.25) | copy-start | bytes 786436

commit v3 on v2

v3 whole, which is shorter than its diff:
```python
import jax
import jax.numpy as jnp
from jax import lax
from jax.experimental import pallas as pl
from jax.experimental.pallas import tpu as pltpu
from jax.sharding import Mesh
from jax.sharding import PartitionSpec as P

HEAD = 128
POOL_DIM = 256
BLOCK = 128
SP_FS = ("sp_0", "sp_1", "fs")
SP = ("sp_0", "sp_1")
SP_TP = ("sp_0", "sp_1", "tp")
EPSILON = 1e-06
MESH = pl.DeviceIdType.MESH
NRECV, NSEND = 77, 64
NZ, NX, NF = 8, 4, 4
WX, WZ, WB, WBX = (256, 256), (256, 128, 384), 384, 128
F32, BF16 = jnp.float32, jnp.bfloat16
NT = (((1,), (1,)), ((), ()))
TN = (((0,), (0,)), ((), ()))


def dot(a, b, dims=(((1,), (0,)), ((), ()))):
    return lax.dot_general(a, b, dims, preferred_element_type=F32)


def pack_state(state, decay):
    high, mid, low = three_parts(decay)
    row = lax.broadcasted_iota(jnp.int32, (16, HEAD), 0)
    tail = jnp.where(row == 0, high, jnp.where(row == 1, mid, jnp.where(row == 2, low, 0.0)))
    return jnp.concatenate([state, tail], axis=0).astype(BF16)


def three_parts(value):
    high = value.astype(BF16).astype(F32)
    rest = value - high
    mid = rest.astype(BF16).astype(F32)
    return high, mid, rest - mid


def unpack_state(packed):
    whole = packed.astype(F32)
    decay = jnp.sum(whole[HEAD : HEAD + 16], axis=0, keepdims=True)
    return whole[:HEAD], decay


def kernel(
    tok,
    gain,
    wq,
    wf,
    wv,
    wo,
    wp,
    room,
    shift,
    hgain,
    start,
    pmap,
    pscale,
    worec,
    wopool,
    out,
    T,
    GZ1,
    GX2,
    GZ2,
    GX3,
    GZ3,
    GB,
    SH,
    ST,
    K,
    V,
    Q,
    G,
    C,
    QE,
    INS,
    A0,
    SL,
    SR,
    ZS,
    ZR,
    ES,
    ER,
    EXT,
    BS,
    BR,
    RO,
    PO,
    ACT,
    PS,
    PR,
    SC,
    SS,
    iz1,
    ix2,
    iz2,
    ixz3,
    send_sems,
    recv_sems,
):
    z, x = lax.axis_index("sp_0"), lax.axis_index("sp_1")
    f, c = lax.axis_index("fs"), lax.axis_index("tp")
    zat = lambda k: lax.rem(z + (k + NZ), NZ)
    xat = lambda k: lax.rem(x + (k + NX), NX)
    fat = lambda k: lax.rem(f + (k + NF), NF)
    other = 1 - c
    here = z * NX + x
    after = lax.rem(here + 1, NZ * NX)
    ahead = lax.rem(here + NZ * NX - 1, NZ * NX)
    nxt = {"sp_0": after // NX, "sp_1": lax.rem(after, NX)}
    prv = {"sp_0": ahead // NX, "sp_1": lax.rem(ahead, NX)}

    barrier = pltpu.get_barrier_semaphore()
    met = [{"tp": other}, nxt, prv]
    met += [{"fs": fat(k)} for k in (1, 2, 3)] + [{"sp_1": xat(k)} for k in (1, 2, 3)]
    met += [{"sp_0": zat(k)} for k in range(1, NZ)]
    for who in met:
        pl.semaphore_signal(barrier, inc=1, device_id=who, device_id_type=MESH)

    count = [0]
    sent = []

    def sem():
        count[0] += 1
        assert count[0] <= NRECV
        return count[0] - 1

    def copy(n, src, dst, who, slot=0):
        return pltpu.make_async_remote_copy(
            src_ref=src,
            dst_ref=dst,
            send_sem=send_sems.at[slot],
            recv_sem=recv_sems.at[n],
            device_id=who,
            device_id_type=MESH,
        )

    def send(n, src, dst, who):
        slot = len(sent) % NSEND
        if len(sent) >= NSEND:
            sent[-NSEND].wait_send()
        made = copy(n, src, dst, who, slot)
        made.start()
        sent.append(made)

    def landed(n, dst):
        copy(n, dst, dst, {"tp": other}).wait_recv()

    rank = here * NF + f
    row = lax.broadcasted_iota(jnp.int32, (16, 128), 0)
    lane = lax.broadcasted_iota(jnp.int32, (16, 128), 1)
    gains = jnp.broadcast_to(gain[pl.ds(rank // 8, 1), :], (16, 128))
    gains = jnp.where(lane == lax.rem(rank, 8) * 16 + row, gains, 0.0)
    gains = jnp.sum(gains, axis=1, keepdims=True)
    weights = [(w[...].astype(F32) * gains).astype(BF16) for w in (wf, wv, wq, wo)]
    folded = [dot(wp[:, 256 * i : 256 * i + 256], pmap[i]) for i in range(2)]
    weights.append((jnp.concatenate(folded, axis=1) * gains * pscale[...]).astype(BF16))
    eye = jnp.where(lane[:, :16] == row[:, :16], 1.0, 0.0).astype(BF16)
    turned = [dot(eye, w[...], NT).astype(BF16) for w in (worec, wopool)]
    turned = jnp.concatenate(turned, axis=1)
    for i in range(NF):
        chunk = [w[:, 128 * i : 128 * i + 128] for w in weights]
        iz1[i] = jnp.concatenate(chunk[:2], axis=1)
        ix2[i] = jnp.concatenate(chunk[2:4], axis=1)
        iz2[i] = chunk[4]
    ixz3[...] = turned[:, :640]
    mine = pl.ds(pl.multiple_of(f * 16, 16), 16)
    pieces = ((GZ1, iz1), (GX2, ix2), (GZ2, iz2))
    for buffer, own in pieces:
        buffer[z, x, mine, :] = own[f]
    GX3[z, x, mine, :] = turned[:, :256]
    GZ3[z, x, mine, :] = turned[:, 256:640]
    GB[z, x, mine, :] = turned[:, 640:]
    T[c, f] = tok[...]
    SH[f] = jnp.transpose(shift[...])
    for i in range(NF):
        SS[i] = jnp.transpose(start[0, i]).astype(BF16)

    pl.semaphore_wait(barrier, len(met))

    def over_y(pairs):
        ns = [sem() for _ in pairs]
        for k in (1, 3, 2):
            to = fat(k)
            for n, (buffer, own) in zip(ns, pairs):
                send(n, own.at[to], buffer.at[z, x, mine, :], {"fs": to})
        return [(n, buffer.at[z, x, pl.ds(0, 48), :]) for n, (buffer, _) in zip(ns, pairs)]

    def over_out():
        ns = sem(), sem()
        for k in (1, 3, 2):
            to = {"fs": fat(k)}
            send(ns[0], ixz3.at[:, pl.ds(0, 256)], GX3.at[z, x, mine, :], to)
            send(ns[1], ixz3.at[:, pl.ds(256, 384)], GZ3.at[z, x, mine, :], to)
        return [(n, b.at[z, x, pl.ds(0, 48), :]) for n, b in zip(ns, (GX3, GZ3))]

    y1 = over_y(pieces[:1])
    y2 = over_y(pieces[1:3])
    y3 = over_out()
    nshift = sem()
    for k in (1, 3, 2):
        send(nshift, SH.at[f], SH.at[f], {"fs": fat(k)})

    first, second = pl.ds(0, 128), pl.ds(128, 128)
    right, left = {"fs": fat(1)}, {"fs": fat(3)}
    nt = [sem() for _ in range(3)]
    near, far_off = sem(), sem()

    def relay(n, seq, rows):
        send(n, T.at[c, seq, rows, :], T.at[c, seq, rows, :], {"tp": other})

    for i, (a, b) in enumerate(((first, second), (second, first))):
        send(nt[i], tok.at[a, :], T.at[c, f, a, :], right)
        send(nt[i], tok.at[b, :], T.at[c, f, b, :], left)
    send(near, tok, T.at[c, f], {"tp": other})

    def token_steps():
        landed(nt[0], T.at[c, fat(1)])
        send(nt[2], T.at[c, fat(-1), first, :], T.at[c, fat(-1), first, :], right)
        send(nt[2], T.at[c, fat(1), second, :], T.at[c, fat(1), second, :], left)
        relay(near, fat(-1), first)
        relay(near, fat(1), second)
        yield
        landed(nt[1], T.at[c, fat(1)])
        relay(near, fat(-1), second)
        relay(near, fat(1), first)
        yield
        landed(nt[2], T.at[c, fat(2)])
        relay(far_off, fat(2), first)
        relay(far_off, fat(2), second)
        yield

    def plane(waits, vx, vz):
        zr, zl = {"sp_0": zat(1)}, {"sp_0": zat(-1)}
        xr, xl = {"sp_1": xat(1)}, {"sp_1": xat(-1)}
        whole, lowx, highx = pl.ds(0, 4), pl.ds(0, 2), pl.ds(2, 2)
        for w in waits:
            landed(*w)
        if vx:
            xs = sem()
            for k in (1, 3, 2):
                send(xs, vx(z, x), vx(z, x), {"sp_1": xat(k)})
        nz = [sem() for _ in range(4)]
        send(nz[0], vz(z, x), vz(z, x), zr)
        send(nz[0], vz(z, x), vz(z, x), zl)
        forwards = []
        last = sem()

        def spread(offsets):
            n = sem()
            for offset in offsets:
                at = zat(offset)
                send(n, vz(at, x), vz(at, x), xr)
                send(n, vz(at, x), vz(at, x), xl)
            forwards.append((n, offsets))

        def forward(ready):
            for n, offsets in ready:
                landed(n, vz(z, pl.ds(0, 2 * len(offsets))))
                for offset in offsets:
                    at = zat(offset)
                    if 0 <= offset < 4:
                        send(last, vz(at, xat(-1)), vz(at, xat(-1)), xr)
                    else:
                        send(last, vz(at, xat(1)), vz(at, xat(1)), xl)

        spread((0,))
        yield
        if vx:
            landed(xs, vx(z, pl.ds(0, 3)))
            mz = [sem() for _ in range(4)]
            send(mz[0], vx(z, whole), vx(z, whole), zr)
            send(mz[0], vx(z, whole), vx(z, whole), zl)
            yield
        for k in (1, 2, 3):
            back, front = zat(-k), zat(k)
            landed(nz[k - 1], vz(z, pl.ds(0, 2)))
            part = vz(back, x, 1 if k == 3 else 0)
            send(nz[k], part, part, zr)
            part = vz(front, x, 2 if k == 3 else 0)
            send(nz[k], part, part, zl)
            ready = list(forwards)
            forwards.clear()
            spread((-k, k))
            if vx:
                landed(mz[k - 1], vx(pl.ds(0, 2), whole))
                part = vx(back, lowx if k == 3 else whole)
                send(mz[k], part, part, zr)
                part = vx(front, highx if k == 3 else whole)
                send(mz[k], part, part, zl)
            forward(ready)
            yield
        far = zat(4)
        landed(nz[3], vz(far, x))
        spread((4,))
        forward(forwards)
        if vx:
            landed(mz[3], vx(far, whole))
        yield
        landed(last, vz(pl.ds(0, NZ), x))
        yield

    def views(GX, GZ):
        halves = (None, pl.ds(0, 32), pl.ds(32, 32))

        def vz(zi, xi, part=0):
            return GZ.at[zi, xi, halves[part], :] if part else GZ.at[zi, xi]

        return (GX is not None) and (lambda zi, xi: GX.at[zi, xi]), vz

    lanes = (pl.ds(WBX, WB - WBX), pl.ds(WBX, 128), pl.ds(WBX + 128, 128))
    late = plane(
        (),
        lambda zi, xi: GB.at[zi, xi, mine, pl.ds(0, WBX)],
        lambda zi, xi, part=0: GB.at[zi, xi, mine, lanes[part]],
    )

    def late_over_y():
        first, second = pl.ds(0, 4), pl.ds(4, 4)

        def part(k, half):
            rows = pl.ds(pl.multiple_of(fat(k) * 16, 16), 16)
            return GB.at[half, :, rows, :]

        near, far = sem(), sem()
        for n, (a, b) in ((near, (first, second)), (far, (second, first))):
            send(n, part(0, a), part(0, a), right)
            send(n, part(0, b), part(0, b), left)
        yield
        landed(near, part(0, pl.ds(0, NZ)))
        send(far, part(-1, first), part(-1, first), right)
        send(far, part(1, second), part(1, second), left)
        yield
        landed(far, GB.at[:, :, pl.ds(0, 32), :])
        yield

    one = plane(y1, *views(None, GZ1))
    two = plane(y2, *views(GX2, GZ2))
    three = plane(y3, *views(GX3, GZ3))
    tokens = token_steps()

    ns = sem()

    def start_copies():
        return [copy(ns, SS.at[fat(k)], ST, {"fs": fat(k)}, NSEND + i) for i, k in enumerate((1, 2, 3))]

    @pl.when(f == x)
    def _():
        ST[...] = SS[f]
        for made in start_copies():
            made.start()

    next(late)
    next(one)
    next(two)
    next(late)
    next(one)
    next(tokens)
    next(one)
    next(two)
    next(late)
    next(one)
    next(tokens)
    next(one)
    next(late)
    next(two)
    next(three)
    next(one)
    landed(near, T.at[other, pl.ds(0, 3)])
    landed(nshift, SH.at[pl.ds(0, 3)])

    i0 = lax.broadcasted_iota(jnp.int32, (BLOCK, BLOCK), 0)
    i1 = lax.broadcasted_iota(jnp.int32, (BLOCK, BLOCK), 1)
    causal = i0 >= i1
    tril = jnp.where(causal, 1.0, 0.0).astype(BF16)
    ones = jnp.ones((BLOCK, BLOCK), BF16)
    my_room = room[pl.ds(f, 1), :]

    half = NZ // 2

    def each(body):
        for s in range(4):
            body(s, 0)

    def through(s, *weights):
        low = jnp.concatenate([w[:half].reshape(1024, w.shape[-1]) for w in weights], axis=1)
        high = jnp.concatenate([w[half:].reshape(1024, w.shape[-1]) for w in weights], axis=1)
        return (dot(T[0, s], low) + dot(T[1, s], high)) * SC[s]

    def project(s, _):
        w0, w1 = T[0, s].astype(F32), T[1, s].astype(F32)
        square = jnp.sum(w0 * w0 + w1 * w1, axis=1, keepdims=True)
        SC[s] = lax.rsqrt(square * (1.0 / 2048) + EPSILON)
        both = through(s, GZ1)
        keys = my_room * jax.nn.sigmoid(-both[:, :128])
        K[s] = keys
        value = both[:, 128:].astype(BF16)
        V[s] = value
        lag = SH[s, pl.ds(f, 1), :]
        ends, adds = [], []
        for b in range(2):
            rows = slice(b * BLOCK, (b + 1) * BLOCK)
            lags = three_parts(lag[:, rows])
            spread = [jnp.where(causal, jnp.broadcast_to(p, (BLOCK, BLOCK)), 0.0).astype(BF16) for p in lags]
            parts = [p.astype(BF16) for p in three_parts(jnp.log1p(-keys[rows]))]
            within = dot(
                jnp.concatenate([tril] * 3 + spread, axis=1),
                jnp.concatenate(parts + [ones] * 3, axis=0),
            )
            C[s, rows, :] = within
            end = within[BLOCK - 1 :]
            adds.append(dot(value[rows], (keys[rows] * jnp.exp(end - within)).astype(BF16), TN))
            ends.append(end)
        A0[s] = adds[0]
        SL[s] = pack_state(jnp.exp(ends[1]) * adds[0] + adds[1], ends[0] + ends[1])
        return 0

    for k in (0, -1, 1):
        project(fat(k), 0)
    next(two)
    next(three)
    next(late)
    next(tokens)
    landed(far_off, T.at[other, 0])
    project(fat(2), 0)

    def project_rest(s, _):
        rest = through(s, GX2, GZ2)
        query = rest[:, :128]
        Q[s] = query * jax.nn.sigmoid(query) * HEAD ** (-0.5)
        gate = rest[:, 128:256]
        G[s] = gate * jax.nn.sigmoid(gate) * hgain[...]
        pool = rest[:, 256:].astype(BF16)
        EXT[s, 128:384, :] = pool
        BS[s] = pool[240:256]
        return 0

    sx = sem()
    SR[x] = SL[x]
    for k in (1, 3, 2):
        send(sx, SL.at[xat(k)], SR.at[x], {"sp_1": xat(k)})
    next(two)
    next(late)
    next(three)
    landed(sx, SR.at[pl.ds(0, 3)])
    state, decay = unpack_state(SR[0])
    for i in range(1, NX):
        later, fade = unpack_state(SR[i])
        state, decay = jnp.exp(fade) * state + later, decay + fade
    ZS[...] = pack_state(state, decay)
    sz = sem()
    for k in (4, 3, 5, 2, 6, 1, 7):
        send(sz, ZS, ZR.at[z], {"sp_0": zat(k)})
    next(two)
    next(late)
    late = late_over_y()
    next(late)
    next(two)
    each(project_rest)
    nb = sem()
    send(nb, BS, BR, nxt)

    def inner(s, _):
        for b in range(2):
            rows = slice(b * BLOCK, (b + 1) * BLOCK)
            within = C[s, rows, :]
            centre = within[BLOCK // 2 - 1 : BLOCK // 2]
            query, keys = Q[s, rows, :], K[s, rows, :]
            scores = dot(
                (query * jnp.exp(within - centre)).astype(BF16),
                (keys * jnp.exp(centre - within)).astype(BF16),
                NT,
            )
            scores = jnp.where(causal, scores, 0.0).astype(BF16)
            INS[s, rows, :] = dot(scores, V[s, rows, :])
            QE[s, rows, :] = (query * jnp.exp(within)).astype(BF16)
        return 0

    each(inner)
    next(three)
    next(late)

    landed(nb, BR)
    span = lax.shift_left(jnp.int32(2), c * 2 + f // 2)
    ti = lax.broadcasted_iota(jnp.int32, (256, 384), 0)
    si = lax.broadcasted_iota(jnp.int32, (256, 384), 1) - 128
    band = jnp.where((si <= ti) & (si > ti - span) & (si >= -16), 1.0, 0.0).astype(BF16)
    position = here * 256 + lax.broadcasted_iota(jnp.int32, (256, 128), 0)
    amount = jnp.minimum(position + 1, span).astype(F32)

    def pool(s, _):
        EXT[s, 0:128, :] = jnp.zeros((128, 128), BF16)

        @pl.when(here > 0)
        def _():
            EXT[s, 112:128, :] = BR[s]

        window = dot(band, EXT[s])
        PO[s] = (window / amount - EXT[s, 128:384, :].astype(F32)).astype(BF16)
        return 0

    each(pool)

    def give_back(buffer, slot):
        n = sem()
        ACT[slot + f] = buffer[f]
        for k in (1, 3, 2):
            send(n, buffer.at[fat(k)], ACT.at[slot + f], {"fs": fat(k)})
        return n

    given_pool = give_back(PO, 4)

    landed(sz, ZR.at[pl.ds(0, NZ - 1)])

    @pl.when(f != x)
    def _():
        landed(ns, ST)

    def pass_z(i, state):
        later, fade = unpack_state(ZR[i])
        return jnp.exp(fade) * state + later

    state = lax.fori_loop(0, z, pass_z, ST[...].astype(F32))
    for i in range(NX):
        ES[i] = state.astype(BF16)
        if i < NX - 1:
            later, fade = unpack_state(SR[i])
            state = jnp.exp(fade) * state + later
    sb = sem()
    ER[x] = ES[x]
    for k in (1, 3, 2):
        send(sb, ES.at[xat(k)], ER.at[x], {"sp_1": xat(k)})
    next(three)
    landed(sb, ER.at[pl.ds(0, 3)])

    def finish(s, _):
        entering = ER[s].astype(F32)
        middle = jnp.exp(C[s, BLOCK - 1 : BLOCK, :]) * entering + A0[s]
        for b, state in enumerate((ER[s], middle.astype(BF16))):
            rows = slice(b * BLOCK, (b + 1) * BLOCK)
            raw = INS[s, rows, :] + dot(QE[s, rows, :], state, NT)
            square = jnp.mean(raw * raw, axis=1, keepdims=True)
            RO[s, rows, :] = (raw * lax.rsqrt(square + EPSILON) * G[s, rows, :]).astype(BF16)
        return 0

    each(finish)
    given_rec = give_back(RO, 0)
    next(three)
    next(three)
    next(late)
    landed(given_pool, ACT.at[pl.ds(0, 3)])
    landed(given_rec, ACT.at[pl.ds(0, 3)])

    a, b, d = (
        jnp.concatenate([ACT[i] for i in range(*span)], axis=1) for span in ((0, 2), (2, 5), (5, 8))
    )
    my_rows = pl.ds(pl.multiple_of(c * 128, 128), 128)
    their_rows = pl.ds(pl.multiple_of(other * 128, 128), 128)
    swap = sem()
    for i in range(4):
        at, cols = slice(2 * i, 2 * i + 2), slice(512 * i, 512 * i + 512)
        total = dot(a, GX3[at].reshape(512, 256), NT)
        total += dot(b, GZ3[at].reshape(512, WZ[2]), NT)
        total += dot(d, GB[at].reshape(512, WB), NT)
        PS[:, cols] = total.astype(BF16)
        send(swap, PS.at[their_rows, pl.ds(512 * i, 512)], PR.at[:, pl.ds(512 * i, 512)], {"tp": other})
    landed(swap, PR)
    out[...] = (PS[my_rows, :].astype(F32) + PR[...].astype(F32)).astype(BF16)

    for made in sent[-NSEND:]:
        made.wait_send()

    @pl.when(f == x)
    def _():
        for made in start_copies():
            made.wait_send()


def per_device(
    tokens,
    norm_gain,
    query_weight,
    forget_weight,
    value_weight,
    outgate_weight,
    pool_in_weight,
    forget_room,
    decay_shift,
    head_gain,
    start_state,
    pool_map,
    pool_scale,
    out_rec_weight,
    out_pool_weight,
):
    vmem = lambda *shape: pltpu.VMEM(shape, F32)
    half = lambda *shape: pltpu.VMEM(shape, BF16)
    mixed = pl.pallas_call(
        kernel,
        out_shape=jax.ShapeDtypeStruct((128, 2048), BF16),
        in_specs=[pl.BlockSpec(memory_space=pltpu.VMEM)] * 15,
        out_specs=pl.BlockSpec(memory_space=pltpu.VMEM),
        scratch_shapes=[
            half(2, 4, 256, 1024),
            half(NZ, NX, 64, WZ[0]),
            half(NZ, NX, 64, WX[0]),
            half(NZ, NX, 64, WZ[1]),
            half(NZ, NX, 64, WX[1]),
            half(NZ, NX, 64, WZ[2]),
            half(NZ, NX, 64, WB),
            vmem(4, 4, 256),
            half(128, 128),
            vmem(4, 256, 128),
            half(4, 256, 128),
            vmem(4, 256, 128),
            vmem(4, 256, 128),
            vmem(4, 256, 128),
            half(4, 256, 128),
            vmem(4, 256, 128),
            vmem(4, 128, 128),
            half(4, 144, 128),
            half(4, 144, 128),
            half(144, 128),
            half(NZ, 144, 128),
            half(4, 128, 128),
            half(4, 128, 128),
            half(4, 384, 128),
            half(4, 16, 128),
            half(4, 16, 128),
            half(4, 256, 128),
            half(4, 256, 128),
            half(8, 256, 128),
            half(256, 2048),
            half(128, 2048),
            vmem(4, 256, 1),
            half(4, 128, 128),
            half(4, 16, 256),
            half(4, 16, 256),
            half(4, 16, 128),
            half(16, 640),
            pltpu.SemaphoreType.DMA((NSEND + 3,)),
            pltpu.SemaphoreType.DMA((NRECV,)),
        ],
        compiler_params=pltpu.CompilerParams(
            collective_id=0, has_side_effects=True, vmem_limit_bytes=60 * 1024 * 1024
        ),
    )(
        tokens[0],
        norm_gain.reshape(16, 128),
        query_weight,
        forget_weight,
        value_weight,
        outgate_weight,
        pool_in_weight,
        forget_room.reshape(4, 128),
        decay_shift[0],
        head_gain.reshape(1, 128),
        start_state,
        pool_map,
        pool_scale.reshape(1, 512),
        out_rec_weight,
        out_pool_weight,
    )
    return mixed[None]


def solution(mesh):
    finer = Mesh(
        mesh.devices.reshape(8, 4, mesh.shape["fs"], mesh.shape["tp"]), ("sp_0", "sp_1", "fs", "tp")
    )
    placed = (
        P("fs", SP, "tp"),
        P(),
        P(SP_FS, "tp"),
        P(SP_FS, "tp"),
        P(SP_FS, "tp"),
        P(SP_FS, "tp"),
        P(SP_FS, "tp"),
        P("tp"),
        P("fs", SP, "tp"),
        P(),
        P("fs", "tp", None, None),
        P("tp", None, None),
        P("tp"),
        P("tp", SP_FS),
        P("tp", SP_FS),
    )
    return jax.shard_map(
        per_device, mesh=finer, in_specs=placed, out_specs=P("fs", SP_TP, None), check_vma=False
    )
```

time: 93.9 us -> 87 us (0.927)
  Pallas kernels: 84.8 us -> 81.9 us
  other arithmetic: 1.97 us -> 0 us
  local copies, waits for them, and re-layouts: 6.67 us -> 4.87 us
    pallas_call x1, Pallas kernels: 84.8 us -> 81.9 us  [per_device(): pl.pallas_call(kernel, out_shape=jax.ShapeDtypeStruct((128, 2048), BF16),...]
    unnamed x24 -> x10, local copies, waits for them, and re-layouts: 3.37 us -> 4.87 us
    broadcast_in_dim x2 -> x0, local copies, waits for them, and re-layouts: 1.22 us -> none  [per_device(): out_all = jnp.broadcast_to(out_t[None], (4, 16, 1024))]
    concatenate x2 -> x0, other arithmetic: 1.21 us -> none  [the longest x1 0.61 us: per_device(): jnp.concatenate([scaled(query_weight), scaled(outgate_weight)], axis=2)]
where the time goes in v3:
time: 87 us; the launch traced here: 86.8 us
  Pallas kernels  81.9 us (94%)
  local copies, waits for them, and re-layouts  4.87 us (6%)
    pallas_call x1, Pallas kernels, per_device(): pl.pallas_call(kernel, out_shape=jax.ShapeDtypeStruct((128, 2048), BF16),...  81.9 us
    unnamed x10, local copies, waits for them, and re-layouts  4.87 us

profile of v3, /device:TPU:1, one launch (start us, length us, event | category | flops | bytes accessed | tf_op | source)
XLA Modules:
  0.0 86.8 jit_solution(7827936897785419028)
XLA Ops:
  0.0 0.0 copy-start.2
  0.0 0.7 copy-done.2
  0.7 0.0 copy-start
  0.7 0.8 copy.16
  1.5 0.0 copy-done
  1.5 0.0 copy-start.1
  1.5 0.8 copy.17.worec
  2.2 0.0 copy-done.1
  2.2 0.7 copy.18.wopool
  3.0 81.9 %shard_map.145 = bf16[128,2048]{1,0:T(8,128)(2,1)} custom-call(bf16[256,1024]{1,0:T(8,128)(2,1)} %bitcast.8, f32[16,128]{1,0:T(8,128)} %bitcast.10, bf16[16,512]{1,0:T(8,128)(2,1)} %wq.1, bf16[16,512]{1,0:T(8,128)(2,1)} %wf.1, bf16[16,512]{1,0:T(8,128)(2,1)} %wv.1, bf16[16,512]{1,0:T(8,128)(2,1)} %wo.1, bf16[16,512]{1,0:T(8,128)(2,1)} %wp.1, ...), custom_call_target="tpu_custom_call" | custom-call | tf_op jit(solution)/shard_map/pallas_call | solution.py:603
  84.9 1.9 %copy.20 = bf16[1,128,2048]{2,1,0:T(8,128)(2,1)} copy(bf16[1,128,2048]{2,1,0:T(8,128)(2,1)} %bitcast.7) | data formatting | bytes 1048576
Async XLA Ops:
  0.0 0.7 copy-start.2
  0.7 0.8 copy-start
  1.5 0.8 copy-start.1

commit v4 on v3

--- a/solution.py
+++ b/solution.py
@@ -1,3 +1,5 @@
+import functools
+
 import jax
 import jax.numpy as jnp
 from jax import lax
@@ -14,6 +16,14 @@
 SP_TP = ("sp_0", "sp_1", "tp")
 EPSILON = 1e-06
 MESH = pl.DeviceIdType.MESH
+ORDER = (
+    "LZ0", "LZ1", "LF0", "1Z0", "2Z0", "3Z0", "LZ2", "1Z1", "1Z2", "T1", "LX0", "3X0", "1F0", "2X0",
+    "1Z3", "1Z4", "2Z1", "1F1", "LZ3", "LX1", "1F2", "T2", "1F3", "SQ", "1F4", "3X1", "3F0", "3Z1",
+    "2X1", "LF1", "LF2", "LF3", "LZ4", "T3", "LX2", "1L", "PR3", "PR1", "2Z2", "3Z2", "3F1", "LF4",
+    "2X2", "LX3", "2Z3", "3Z3", "SUMX", "2F0", "2X3", "LX4", "2Z4", "LL", "Y0", "2F1", "2F2", "3Z4",
+    "3F2", "2F3", "3X2", "3F3", "2F4", "3F4", "Y1", "PASSZ", "2L", "2X4", "REST", "3L", "INNER",
+    "FIN", "3X3", "POOL", "Y2", "3X4",
+)
 NRECV, NSEND = 77, 64
 NZ, NX, NF = 8, 4, 4
 WX, WZ, WB, WBX = (256, 256), (256, 128, 384), 384, 128
@@ -219,91 +229,87 @@
         send(nt[i], tok.at[b, :], T.at[c, f, b, :], left)
     send(near, tok, T.at[c, f], {"tp": other})
 
-    def token_steps():
+    def tokens_1():
         landed(nt[0], T.at[c, fat(1)])
         send(nt[2], T.at[c, fat(-1), first, :], T.at[c, fat(-1), first, :], right)
         send(nt[2], T.at[c, fat(1), second, :], T.at[c, fat(1), second, :], left)
         relay(near, fat(-1), first)
         relay(near, fat(1), second)
-        yield
+
+    def tokens_2():
         landed(nt[1], T.at[c, fat(1)])
         relay(near, fat(-1), second)
         relay(near, fat(1), first)
-        yield
+
+    def tokens_3():
         landed(nt[2], T.at[c, fat(2)])
         relay(far_off, fat(2), first)
         relay(far_off, fat(2), second)
-        yield
-
-    def plane(waits, vx, vz):
+
+    steps = {"T1": tokens_1, "T2": tokens_2, "T3": tokens_3}
+
+    def plane(name, waits, vx, vz, direct=False):
         zr, zl = {"sp_0": zat(1)}, {"sp_0": zat(-1)}
         xr, xl = {"sp_1": xat(1)}, {"sp_1": xat(-1)}
         whole, lowx, highx = pl.ds(0, 4), pl.ds(0, 2), pl.ds(2, 2)
-        for w in waits:
-            landed(*w)
+        nz, ns, last = [sem() for _ in range(4)], [sem() for _ in range(5)], sem()
         if vx:
-            xs = sem()
-            for k in (1, 3, 2):
-                send(xs, vx(z, x), vx(z, x), {"sp_1": xat(k)})
-        nz = [sem() for _ in range(4)]
-        send(nz[0], vz(z, x), vz(z, x), zr)
-        send(nz[0], vz(z, x), vz(z, x), zl)
-        forwards = []
-        last = sem()
-
-        def spread(offsets):
-            n = sem()
-            for offset in offsets:
+            xs, mz = sem(), [sem() for _ in range(4)]
+        offsets = ((0,), (-1, 1), (-2, 2), (-3, 3), (4,))
+
+        def spread(k):
+            for offset in offsets[k]:
                 at = zat(offset)
-                send(n, vz(at, x), vz(at, x), xr)
-                send(n, vz(at, x), vz(at, x), xl)
-            forwards.append((n, offsets))
-
-        def forward(ready):
-            for n, offsets in ready:
-                landed(n, vz(z, pl.ds(0, 2 * len(offsets))))
-                for offset in offsets:
-                    at = zat(offset)
-                    if 0 <= offset < 4:
-                        send(last, vz(at, xat(-1)), vz(at, xat(-1)), xr)
-                    else:
-                        send(last, vz(at, xat(1)), vz(at, xat(1)), xl)
-
-        spread((0,))
-        yield
-        if vx:
-            landed(xs, vx(z, pl.ds(0, 3)))
-            mz = [sem() for _ in range(4)]
-            send(mz[0], vx(z, whole), vx(z, whole), zr)
-            send(mz[0], vx(z, whole), vx(z, whole), zl)
-            yield
-        for k in (1, 2, 3):
-            back, front = zat(-k), zat(k)
-            landed(nz[k - 1], vz(z, pl.ds(0, 2)))
-            part = vz(back, x, 1 if k == 3 else 0)
-            send(nz[k], part, part, zr)
-            part = vz(front, x, 2 if k == 3 else 0)
-            send(nz[k], part, part, zl)
-            ready = list(forwards)
-            forwards.clear()
-            spread((-k, k))
+                send(ns[k], vz(at, x), vz(at, x), xr)
+                send(ns[k], vz(at, x), vz(at, x), xl)
+
+        def z_step(k):
+            if k == 0:
+                for w in waits:
+                    landed(*w)
+                if vx:
+                    for i in (1, 3, 2):
+                        send(xs, vx(z, x), vx(z, x), {"sp_1": xat(i)})
+                for i in (1, 2, 4, 3) if direct else (1,):
+                    for step in (i, -i) if i < 4 else (i,):
+                        send(nz[i - 1], vz(z, x), vz(z, x), {"sp_0": zat(step)})
+            else:
+                landed(nz[k - 1], vz(z, pl.ds(0, 2)) if k < 4 else vz(z, x))
+                if k < 4 and not direct:
+                    part = vz(zat(-k), x, 1 if k == 3 else 0)
+                    send(nz[k], part, part, zr)
+                    part = vz(zat(k), x, 2 if k == 3 else 0)
+                    send(nz[k], part, part, zl)
+            spread(k)
+
+        def x_step(k):
+            if k == 0:
+                landed(xs, vx(z, pl.ds(0, 3)))
+                send(mz[0], vx(z, whole), vx(z, whole), zr)
+                send(mz[0], vx(z, whole), vx(z, whole), zl)
+                return
+            landed(mz[k - 1], vx(pl.ds(0, 2), whole) if k < 4 else vx(z, whole))
+            if k < 4:
+                part = vx(zat(-k), lowx if k == 3 else whole)
+                send(mz[k], part, part, zr)
+                part = vx(zat(k), highx if k == 3 else whole)
+                send(mz[k], part, part, zl)
+
+        def f_step(k):
+            landed(ns[k], vz(z, pl.ds(0, 2 * len(offsets[k]))))
+            for offset in offsets[k]:
+                at = zat(offset)
+                if 0 <= offset < 4:
+                    send(last, vz(at, xat(-1)), vz(at, xat(-1)), xr)
+                else:
+                    send(last, vz(at, xat(1)), vz(at, xat(1)), xl)
+
+        for k in range(5):
+            steps[f"{name}Z{k}"] = functools.partial(z_step, k)
+            steps[f"{name}F{k}"] = functools.partial(f_step, k)
             if vx:
-                landed(mz[k - 1], vx(pl.ds(0, 2), whole))
-                part = vx(back, lowx if k == 3 else whole)
-                send(mz[k], part, part, zr)
-                part = vx(front, highx if k == 3 else whole)
-                send(mz[k], part, part, zl)
-            forward(ready)
-            yield
-        far = zat(4)
-        landed(nz[3], vz(far, x))
-        spread((4,))
-        forward(forwards)
-        if vx:
-            landed(mz[3], vx(far, whole))
-        yield
-        landed(last, vz(pl.ds(0, NZ), x))
-        yield
+                steps[f"{name}X{k}"] = functools.partial(x_step, k)
+        steps[f"{name}L"] = lambda: landed(last, vz(pl.ds(0, NZ), x))
 
     def views(GX, GZ):
         halves = (None, pl.ds(0, 32), pl.ds(32, 32))
@@ -314,35 +320,37 @@
         return (GX is not None) and (lambda zi, xi: GX.at[zi, xi]), vz
 
     lanes = (pl.ds(WBX, WB - WBX), pl.ds(WBX, 128), pl.ds(WBX + 128, 128))
-    late = plane(
+    plane(
+        "L",
         (),
         lambda zi, xi: GB.at[zi, xi, mine, pl.ds(0, WBX)],
         lambda zi, xi, part=0: GB.at[zi, xi, mine, lanes[part]],
     )
 
-    def late_over_y():
-        first, second = pl.ds(0, 4), pl.ds(4, 4)
-
-        def part(k, half):
-            rows = pl.ds(pl.multiple_of(fat(k) * 16, 16), 16)
-            return GB.at[half, :, rows, :]
-
-        near, far = sem(), sem()
-        for n, (a, b) in ((near, (first, second)), (far, (second, first))):
-            send(n, part(0, a), part(0, a), right)
-            send(n, part(0, b), part(0, b), left)
-        yield
-        landed(near, part(0, pl.ds(0, NZ)))
-        send(far, part(-1, first), part(-1, first), right)
-        send(far, part(1, second), part(1, second), left)
-        yield
-        landed(far, GB.at[:, :, pl.ds(0, 32), :])
-        yield
-
-    one = plane(y1, *views(None, GZ1))
-    two = plane(y2, *views(GX2, GZ2))
-    three = plane(y3, *views(GX3, GZ3))
-    tokens = token_steps()
+    half_z, other_half = pl.ds(0, 4), pl.ds(4, 4)
+    ny = sem(), sem()
+
+    def late_part(k, half):
+        rows = pl.ds(pl.multiple_of(fat(k) * 16, 16), 16)
+        return GB.at[half, :, rows, :]
+
+    def late_y0():
+        for n, (a, b) in zip(ny, ((half_z, other_half), (other_half, half_z))):
+            send(n, late_part(0, a), late_part(0, a), right)
+            send(n, late_part(0, b), late_part(0, b), left)
+
+    def late_y1():
+        landed(ny[0], late_part(0, pl.ds(0, NZ)))
+        send(ny[1], late_part(-1, half_z), late_part(-1, half_z), right)
+        send(ny[1], late_part(1, other_half), late_part(1, other_half), left)
+
+    def late_y2():
+        landed(ny[1], GB.at[:, :, pl.ds(0, 32), :])
+
+    steps.update(Y0=late_y0, Y1=late_y1, Y2=late_y2)
+    plane("1", y1, *views(None, GZ1), direct=True)
+    plane("2", y2, *views(GX2, GZ2))
+    plane("3", y3, *views(GX3, GZ3))
 
     ns = sem()
 
@@ -355,24 +363,10 @@
         for made in start_copies():
             made.start()
 
-    next(late)
-    next(one)
-    next(two)
-    next(late)
-    next(one)
-    next(tokens)
-    next(one)
-    next(two)
-    next(late)
-    next(one)
-    next(tokens)
-    next(one)
-    next(late)
-    next(two)
-    next(three)
-    next(one)
-    landed(near, T.at[other, pl.ds(0, 3)])
-    landed(nshift, SH.at[pl.ds(0, 3)])
+    def squares(s):
+        w0, w1 = T[0, s].astype(F32), T[1, s].astype(F32)
+        square = jnp.sum(w0 * w0 + w1 * w1, axis=1, keepdims=True)
+        SC[s] = lax.rsqrt(square * (1.0 / 2048) + EPSILON)
 
     i0 = lax.broadcasted_iota(jnp.int32, (BLOCK, BLOCK), 0)
     i1 = lax.broadcasted_iota(jnp.int32, (BLOCK, BLOCK), 1)
@@ -393,9 +387,6 @@
         return (dot(T[0, s], low) + dot(T[1, s], high)) * SC[s]
 
     def project(s, _):
-        w0, w1 = T[0, s].astype(F32), T[1, s].astype(F32)
-        square = jnp.sum(w0 * w0 + w1 * w1, axis=1, keepdims=True)
-        SC[s] = lax.rsqrt(square * (1.0 / 2048) + EPSILON)
         both = through(s, GZ1)
         keys = my_room * jax.nn.sigmoid(-both[:, :128])
         K[s] = keys
@@ -420,14 +411,35 @@
         SL[s] = pack_state(jnp.exp(ends[1]) * adds[0] + adds[1], ends[0] + ends[1])
         return 0
 
-    for k in (0, -1, 1):
-        project(fat(k), 0)
-    next(two)
-    next(three)
-    next(late)
-    next(tokens)
-    landed(far_off, T.at[other, 0])
-    project(fat(2), 0)
+    sx, sz, sb, nb = sem(), sem(), sem(), sem()
+
+    def squares_near():
+        landed(near, T.at[other, pl.ds(0, 3)])
+        for k in (0, -1, 1):
+            squares(fat(k))
+
+    def project_near():
+        landed(nshift, SH.at[pl.ds(0, 3)])
+        for k in (0, -1, 1):
+            project(fat(k), 0)
+
+    def project_far():
+        landed(far_off, T.at[other, 0])
+        squares(fat(2))
+        project(fat(2), 0)
+        SR[x] = SL[x]
+        for k in (1, 3, 2):
+            send(sx, SL.at[xat(k)], SR.at[x], {"sp_1": xat(k)})
+
+    def total_x():
+        landed(sx, SR.at[pl.ds(0, 3)])
+        state, decay = unpack_state(SR[0])
+        for i in range(1, NX):
+            later, fade = unpack_state(SR[i])
+            state, decay = jnp.exp(fade) * state + later, decay + fade
+        ZS[...] = pack_state(state, decay)
+        for k in (4, 3, 5, 2, 6, 1, 7):
+            send(sz, ZS, ZR.at[z], {"sp_0": zat(k)})
 
     def project_rest(s, _):
         rest = through(s, GX2, GZ2)
@@ -440,30 +452,9 @@
         BS[s] = pool[240:256]
         return 0
 
-    sx = sem()
-    SR[x] = SL[x]
-    for k in (1, 3, 2):
-        send(sx, SL.at[xat(k)], SR.at[x], {"sp_1": xat(k)})
-    next(two)
-    next(late)
-    next(three)
-    landed(sx, SR.at[pl.ds(0, 3)])
-    state, decay = unpack_state(SR[0])
-    for i in range(1, NX):
-        later, fade = unpack_state(SR[i])
-        state, decay = jnp.exp(fade) * state + later, decay + fade
-    ZS[...] = pack_state(state, decay)
-    sz = sem()
-    for k in (4, 3, 5, 2, 6, 1, 7):
-        send(sz, ZS, ZR.at[z], {"sp_0": zat(k)})
-    next(two)
-    next(late)
-    late = late_over_y()
-    next(late)
-    next(two)
-    each(project_rest)
-    nb = sem()
-    send(nb, BS, BR, nxt)
+    def rest():
+        each(project_rest)
+        send(nb, BS, BR, nxt)
 
     def inner(s, _):
         for b in range(2):
@@ -481,11 +472,6 @@
             QE[s, rows, :] = (query * jnp.exp(within)).astype(BF16)
         return 0
 
-    each(inner)
-    next(three)
-    next(late)
-
-    landed(nb, BR)
     span = lax.shift_left(jnp.int32(2), c * 2 + f // 2)
     ti = lax.broadcasted_iota(jnp.int32, (256, 384), 0)
     si = lax.broadcasted_iota(jnp.int32, (256, 384), 1) - 128
@@ -504,8 +490,6 @@
         PO[s] = (window / amount - EXT[s, 128:384, :].astype(F32)).astype(BF16)
         return 0
 
-    each(pool)
-
     def give_back(buffer, slot):
         n = sem()
         ACT[slot + f] = buffer[f]
@@ -513,30 +497,33 @@
             send(n, buffer.at[fat(k)], ACT.at[slot + f], {"fs": fat(k)})
         return n
 
-    given_pool = give_back(PO, 4)
-
-    landed(sz, ZR.at[pl.ds(0, NZ - 1)])
-
-    @pl.when(f != x)
-    def _():
-        landed(ns, ST)
+    given = []
+
+    def pooling():
+        landed(nb, BR)
+        each(pool)
+        given.append(give_back(PO, 4))
 
     def pass_z(i, state):
         later, fade = unpack_state(ZR[i])
         return jnp.exp(fade) * state + later
 
-    state = lax.fori_loop(0, z, pass_z, ST[...].astype(F32))
-    for i in range(NX):
-        ES[i] = state.astype(BF16)
-        if i < NX - 1:
-            later, fade = unpack_state(SR[i])
-            state = jnp.exp(fade) * state + later
-    sb = sem()
-    ER[x] = ES[x]
-    for k in (1, 3, 2):
-        send(sb, ES.at[xat(k)], ER.at[x], {"sp_1": xat(k)})
-    next(three)
-    landed(sb, ER.at[pl.ds(0, 3)])
+    def from_z():
+        landed(sz, ZR.at[pl.ds(0, NZ - 1)])
+
+        @pl.when(f != x)
+        def _():
+            landed(ns, ST)
+
+        state = lax.fori_loop(0, z, pass_z, ST[...].astype(F32))
+        for i in range(NX):
+            ES[i] = state.astype(BF16)
+            if i < NX - 1:
+                later, fade = unpack_state(SR[i])
+                state = jnp.exp(fade) * state + later
+        ER[x] = ES[x]
+        for k in (1, 3, 2):
+            send(sb, ES.at[xat(k)], ER.at[x], {"sp_1": xat(k)})
 
     def finish(s, _):
         entering = ER[s].astype(F32)
@@ -548,13 +535,30 @@
             RO[s, rows, :] = (raw * lax.rsqrt(square + EPSILON) * G[s, rows, :]).astype(BF16)
         return 0
 
-    each(finish)
-    given_rec = give_back(RO, 0)
-    next(three)
-    next(three)
-    next(late)
-    landed(given_pool, ACT.at[pl.ds(0, 3)])
-    landed(given_rec, ACT.at[pl.ds(0, 3)])
+    def finishing():
+        landed(sb, ER.at[pl.ds(0, 3)])
+        each(finish)
+        given.append(give_back(RO, 0))
+
+    steps.update(
+        SQ=squares_near,
+        PR3=project_near,
+        PR1=project_far,
+        SUMX=total_x,
+        REST=rest,
+        INNER=lambda: each(inner),
+        POOL=pooling,
+        PASSZ=from_z,
+        FIN=finishing,
+    )
+    order = ORDER
+    assert sorted(order) == sorted(steps)
+    for step in order:
+        with jax.named_scope(step):
+            steps[step]()
+
+    for n in given:
+        landed(n, ACT.at[pl.ds(0, 3)])
 
     a, b, d = (
         jnp.concatenate([ACT[i] for i in range(*span)], axis=1) for span in ((0, 2), (2, 5), (5, 8))

time: 87 us -> 79.4 us (0.913)
  Pallas kernels: 81.9 us -> 74.3 us
    pallas_call x1, Pallas kernels: 81.9 us -> 74.3 us  [per_device(): pl.pallas_call(kernel, out_shape=jax.ShapeDtypeStruct((128, 2048), BF16),...]
where the time goes in v4:
time: 79.4 us; the launch traced here: 79.1 us
  Pallas kernels  74.3 us (94%)
  local copies, waits for them, and re-layouts  4.87 us (6%)
    pallas_call x1, Pallas kernels, per_device(): pl.pallas_call(kernel, out_shape=jax.ShapeDtypeStruct((128, 2048), BF16),...  74.3 us
    unnamed x10, local copies, waits for them, and re-layouts  4.87 us

profile of v4, /device:TPU:1, one launch (start us, length us, event | category | flops | bytes accessed | tf_op | source)
XLA Modules:
  0.0 79.1 jit_solution(10554168195035919434)
XLA Ops:
  0.0 0.0 copy-start.2
  0.0 0.7 copy-done.2
  0.7 0.0 copy-start
  0.7 0.8 %copy.16 = f32[1,256,4]{2,1,0:T(8,128)} copy(f32[1,256,4]{1,2,0:T(4,128)S(1)} %copy-done.2) | data formatting | bytes 8192 | tf_op args[8]
  1.5 0.0 copy-done
  1.5 0.0 copy-start.1
  1.5 0.8 copy.17.worec
  2.2 0.0 copy-done.1
  2.2 0.7 copy.18.wopool
  3.0 74.3 %shard_map.145 = bf16[128,2048]{1,0:T(8,128)(2,1)} custom-call(bf16[256,1024]{1,0:T(8,128)(2,1)} %bitcast.8, f32[16,128]{1,0:T(8,128)} %bitcast.10, bf16[16,512]{1,0:T(8,128)(2,1)} %wq.1, bf16[16,512]{1,0:T(8,128)(2,1)} %wf.1, bf16[16,512]{1,0:T(8,128)(2,1)} %wv.1, bf16[16,512]{1,0:T(8,128)(2,1)} %wo.1, bf16[16,512]{1,0:T(8,128)(2,1)} %wp.1, ...), custom_call_target="tpu_custom_call" | custom-call | tf_op jit(solution)/shard_map/pallas_call | solution.py:607
  77.3 1.9 %copy.20 = bf16[1,128,2048]{2,1,0:T(8,128)(2,1)} copy(bf16[1,128,2048]{2,1,0:T(8,128)(2,1)} %bitcast.7) | data formatting | bytes 1048576
Async XLA Ops:
  0.0 0.7 copy-start.2
  0.7 0.8 %copy-start = (bf16[512,16]{0,1:T(8,128)(2,1)S(1)}, bf16[512,16]{0,1:T(8,128)(2,1)}, u32[]{:S(2)}) copy-start(bf16[512,16]{0,1:T(8,128)(2,1)} %param.28) | copy-start | bytes 49156
  1.5 0.8 copy-start.1

commit v5 on v4

--- a/solution.py
+++ b/solution.py
@@ -17,14 +17,14 @@
 EPSILON = 1e-06
 MESH = pl.DeviceIdType.MESH
 ORDER = (
-    "LZ0", "LZ1", "LF0", "1Z0", "2Z0", "3Z0", "LZ2", "1Z1", "1Z2", "T1", "LX0", "3X0", "1F0", "2X0",
-    "1Z3", "1Z4", "2Z1", "1F1", "LZ3", "LX1", "1F2", "T2", "1F3", "SQ", "1F4", "3X1", "3F0", "3Z1",
-    "2X1", "LF1", "LF2", "LF3", "LZ4", "T3", "LX2", "1L", "PR3", "PR1", "2Z2", "3Z2", "3F1", "LF4",
-    "2X2", "LX3", "2Z3", "3Z3", "SUMX", "2F0", "2X3", "LX4", "2Z4", "LL", "Y0", "2F1", "2F2", "3Z4",
-    "3F2", "2F3", "3X2", "3F3", "2F4", "3F4", "Y1", "PASSZ", "2L", "2X4", "REST", "3L", "INNER",
-    "FIN", "3X3", "POOL", "Y2", "3X4",
+    "LZ0", "LZ1", "LF0", "1Z0", "LX0", "2Z0", "LZ2", "LF1", "1Z1", "1F0", "1Z2", "2X0", "LF2", "T1",
+    "3Z0", "1Z3", "1Z4", "LX1", "2Z1", "LZ3", "T2", "1F1", "1F2", "2X1", "SQ", "1F3", "LX2", "LZ4",
+    "1F4", "3X0", "3Z1", "LF3", "2Z2", "T3", "LF4", "2X2", "1L", "PR3", "PR1", "2Z3", "3X1", "LX3",
+    "LL", "2X3", "3Z2", "2Z4", "SUMX", "3F0", "2F0", "2F1", "2F2", "2F3", "LX4", "Y0", "3F1", "2F4",
+    "3Z3", "2X4", "3F2", "2L", "REST", "Y1", "3X2", "3F3", "INNER", "PASSZ", "POOL", "3Z4", "3X3",
+    "FIN", "Y2", "3F4", "3X4", "3L", "OUTP",
 )
-NRECV, NSEND = 77, 64
+NRECV, NSEND, NLONG = 77, 40, 13
 NZ, NX, NF = 8, 4, 4
 WX, WZ, WB, WBX = (256, 256), (256, 128, 384), 384, 128
 F32, BF16 = jnp.float32, jnp.bfloat16
@@ -106,12 +106,16 @@
     PR,
     SC,
     SS,
+    S0,
+    PM,
+    PT,
     iz1,
     ix2,
     iz2,
     ixz3,
     send_sems,
     recv_sems,
+    local_sems,
 ):
     z, x = lax.axis_index("sp_0"), lax.axis_index("sp_1")
     f, c = lax.axis_index("fs"), lax.axis_index("tp")
@@ -125,6 +129,13 @@
     nxt = {"sp_0": after // NX, "sp_1": lax.rem(after, NX)}
     prv = {"sp_0": ahead // NX, "sp_1": lax.rem(ahead, NX)}
 
+    taken = [
+        pltpu.make_async_copy(source, target, local_sems.at[i])
+        for i, (source, target) in enumerate(((pmap, PM), (tok, T.at[c, 1]), (start.at[0], S0)))
+    ]
+    for made in taken:
+        made.start()
+
     barrier = pltpu.get_barrier_semaphore()
     met = [{"tp": other}, nxt, prv]
     met += [{"fs": fat(k)} for k in (1, 2, 3)] + [{"sp_1": xat(k)} for k in (1, 2, 3)]
@@ -133,7 +144,7 @@
         pl.semaphore_signal(barrier, inc=1, device_id=who, device_id_type=MESH)
 
     count = [0]
-    sent = []
+    sent, sent_long = [], []
 
     def sem():
         count[0] += 1
@@ -150,13 +161,13 @@
             device_id_type=MESH,
         )
 
-    def send(n, src, dst, who):
-        slot = len(sent) % NSEND
-        if len(sent) >= NSEND:
-            sent[-NSEND].wait_send()
-        made = copy(n, src, dst, who, slot)
+    def send(n, src, dst, who, long=False):
+        made_before, slots, base = (sent_long, NLONG, NSEND) if long else (sent, NSEND, 0)
+        if len(made_before) >= slots:
+            made_before[-slots].wait_send()
+        made = copy(n, src, dst, who, base + len(made_before) % slots)
         made.start()
-        sent.append(made)
+        made_before.append(made)
 
     def landed(n, dst):
         copy(n, dst, dst, {"tp": other}).wait_recv()
@@ -167,12 +178,11 @@
     gains = jnp.broadcast_to(gain[pl.ds(rank // 8, 1), :], (16, 128))
     gains = jnp.where(lane == lax.rem(rank, 8) * 16 + row, gains, 0.0)
     gains = jnp.sum(gains, axis=1, keepdims=True)
+    taken[0].wait()
     weights = [(w[...].astype(F32) * gains).astype(BF16) for w in (wf, wv, wq, wo)]
-    folded = [dot(wp[:, 256 * i : 256 * i + 256], pmap[i]) for i in range(2)]
+    folded = [dot(wp[:, 256 * i : 256 * i + 256], PM[i]) for i in range(2)]
     weights.append((jnp.concatenate(folded, axis=1) * gains * pscale[...]).astype(BF16))
-    eye = jnp.where(lane[:, :16] == row[:, :16], 1.0, 0.0).astype(BF16)
-    turned = [dot(eye, w[...], NT).astype(BF16) for w in (worec, wopool)]
-    turned = jnp.concatenate(turned, axis=1)
+    turned = jnp.concatenate([worec[...], wopool[...]], axis=1)
     for i in range(NF):
         chunk = [w[:, 128 * i : 128 * i + 128] for w in weights]
         iz1[i] = jnp.concatenate(chunk[:2], axis=1)
@@ -186,10 +196,8 @@
     GX3[z, x, mine, :] = turned[:, :256]
     GZ3[z, x, mine, :] = turned[:, 256:640]
     GB[z, x, mine, :] = turned[:, 640:]
-    T[c, f] = tok[...]
-    SH[f] = jnp.transpose(shift[...])
-    for i in range(NF):
-        SS[i] = jnp.transpose(start[0, i]).astype(BF16)
+    SH[1] = shift[...]
+    taken[1].wait()
 
     pl.semaphore_wait(barrier, len(met))
 
@@ -214,7 +222,7 @@
     y3 = over_out()
     nshift = sem()
     for k in (1, 3, 2):
-        send(nshift, SH.at[f], SH.at[f], {"fs": fat(k)})
+        send(nshift, SH.at[1], SH.at[(5 - k) % 4], {"fs": fat(k)})
 
     first, second = pl.ds(0, 128), pl.ds(128, 128)
     right, left = {"fs": fat(1)}, {"fs": fat(3)}
@@ -222,29 +230,29 @@
     near, far_off = sem(), sem()
 
     def relay(n, seq, rows):
-        send(n, T.at[c, seq, rows, :], T.at[c, seq, rows, :], {"tp": other})
+        send(n, T.at[c, seq, rows, :], T.at[c, seq, rows, :], {"tp": other}, True)
 
     for i, (a, b) in enumerate(((first, second), (second, first))):
-        send(nt[i], tok.at[a, :], T.at[c, f, a, :], right)
-        send(nt[i], tok.at[b, :], T.at[c, f, b, :], left)
-    send(near, tok, T.at[c, f], {"tp": other})
+        send(nt[i], T.at[c, 1, a, :], T.at[c, 0, a, :], right, True)
+        send(nt[i], T.at[c, 1, b, :], T.at[c, 2, b, :], left, True)
+    send(near, T.at[c, 1], T.at[c, 1], {"tp": other}, True)
 
     def tokens_1():
-        landed(nt[0], T.at[c, fat(1)])
-        send(nt[2], T.at[c, fat(-1), first, :], T.at[c, fat(-1), first, :], right)
-        send(nt[2], T.at[c, fat(1), second, :], T.at[c, fat(1), second, :], left)
-        relay(near, fat(-1), first)
-        relay(near, fat(1), second)
+        landed(nt[0], T.at[c, 0])
+        send(nt[2], T.at[c, 0, first, :], T.at[c, 3, first, :], right, True)
+        send(nt[2], T.at[c, 2, second, :], T.at[c, 3, second, :], left, True)
+        relay(near, 0, first)
+        relay(near, 2, second)
 
     def tokens_2():
-        landed(nt[1], T.at[c, fat(1)])
-        relay(near, fat(-1), second)
-        relay(near, fat(1), first)
+        landed(nt[1], T.at[c, 0])
+        relay(near, 0, second)
+        relay(near, 2, first)
 
     def tokens_3():
-        landed(nt[2], T.at[c, fat(2)])
-        relay(far_off, fat(2), first)
-        relay(far_off, fat(2), second)
+        landed(nt[2], T.at[c, 3])
+        relay(far_off, 3, first)
+        relay(far_off, 3, second)
 
     steps = {"T1": tokens_1, "T2": tokens_2, "T3": tokens_3}
 
@@ -336,13 +344,13 @@
 
     def late_y0():
         for n, (a, b) in zip(ny, ((half_z, other_half), (other_half, half_z))):
-            send(n, late_part(0, a), late_part(0, a), right)
-            send(n, late_part(0, b), late_part(0, b), left)
+            send(n, late_part(0, a), late_part(0, a), right, True)
+            send(n, late_part(0, b), late_part(0, b), left, True)
 
     def late_y1():
         landed(ny[0], late_part(0, pl.ds(0, NZ)))
-        send(ny[1], late_part(-1, half_z), late_part(-1, half_z), right)
-        send(ny[1], late_part(1, other_half), late_part(1, other_half), left)
+        send(ny[1], late_part(-1, half_z), late_part(-1, half_z), right, True)
+        send(ny[1], late_part(1, other_half), late_part(1, other_half), left, True)
 
     def late_y2():
         landed(ny[1], GB.at[:, :, pl.ds(0, 32), :])
@@ -355,10 +363,14 @@
     ns = sem()
 
     def start_copies():
-        return [copy(ns, SS.at[fat(k)], ST, {"fs": fat(k)}, NSEND + i) for i, k in enumerate((1, 2, 3))]
+        return [copy(ns, SS.at[fat(k)], ST, {"fs": fat(k)}, NSEND + NLONG + i) for i, k in enumerate((1, 2, 3))]
+
+    taken[2].wait()
 
     @pl.when(f == x)
     def _():
+        for i in range(NF):
+            SS[i] = jnp.transpose(S0[i]).astype(BF16)
         ST[...] = SS[f]
         for made in start_copies():
             made.start()
@@ -381,13 +393,16 @@
         for s in range(4):
             body(s, 0)
 
-    def through(s, *weights):
+    def through(slots, *weights):
+        count = len(slots) * 256
+        at = slice(slots[0], slots[-1] + 1)
         low = jnp.concatenate([w[:half].reshape(1024, w.shape[-1]) for w in weights], axis=1)
         high = jnp.concatenate([w[half:].reshape(1024, w.shape[-1]) for w in weights], axis=1)
-        return (dot(T[0, s], low) + dot(T[1, s], high)) * SC[s]
-
-    def project(s, _):
-        both = through(s, GZ1)
+        total = dot(T[0, at].reshape(count, 1024), low) + dot(T[1, at].reshape(count, 1024), high)
+        total = total * SC[at].reshape(count, 1)
+        return [total[256 * i : 256 * i + 256] for i in range(len(slots))]
+
+    def project(s, both):
         keys = my_room * jax.nn.sigmoid(-both[:, :128])
         K[s] = keys
         value = both[:, 128:].astype(BF16)
@@ -409,27 +424,27 @@
             ends.append(end)
         A0[s] = adds[0]
         SL[s] = pack_state(jnp.exp(ends[1]) * adds[0] + adds[1], ends[0] + ends[1])
-        return 0
 
     sx, sz, sb, nb = sem(), sem(), sem(), sem()
 
     def squares_near():
         landed(near, T.at[other, pl.ds(0, 3)])
-        for k in (0, -1, 1):
-            squares(fat(k))
+        for s in range(3):
+            squares(s)
 
     def project_near():
         landed(nshift, SH.at[pl.ds(0, 3)])
-        for k in (0, -1, 1):
-            project(fat(k), 0)
+        for s, both in enumerate(through((0, 1, 2), GZ1)):
+            project(s, both)
 
     def project_far():
-        landed(far_off, T.at[other, 0])
-        squares(fat(2))
-        project(fat(2), 0)
-        SR[x] = SL[x]
+        landed(far_off, T.at[other, 3])
+        squares(3)
+        project(3, through((3,), GZ1)[0])
+        slot_of = lambda sequence: lax.rem(sequence - f + (NF + 1), NF)
+        SR[x] = SL[slot_of(x)]
         for k in (1, 3, 2):
-            send(sx, SL.at[xat(k)], SR.at[x], {"sp_1": xat(k)})
+            send(sx, SL.at[slot_of(xat(k))], SR.at[x], {"sp_1": xat(k)})
 
     def total_x():
         landed(sx, SR.at[pl.ds(0, 3)])
@@ -441,8 +456,7 @@
         for k in (4, 3, 5, 2, 6, 1, 7):
             send(sz, ZS, ZR.at[z], {"sp_0": zat(k)})
 
-    def project_rest(s, _):
-        rest = through(s, GX2, GZ2)
+    def project_rest(s, rest):
         query = rest[:, :128]
         Q[s] = query * jax.nn.sigmoid(query) * HEAD ** (-0.5)
         gate = rest[:, 128:256]
@@ -450,10 +464,11 @@
         pool = rest[:, 256:].astype(BF16)
         EXT[s, 128:384, :] = pool
         BS[s] = pool[240:256]
-        return 0
 
     def rest():
-        each(project_rest)
+        for slots in ((0, 1), (2, 3)):
+            for s, projected in zip(slots, through(slots, GX2, GZ2)):
+                project_rest(s, projected)
         send(nb, BS, BR, nxt)
 
     def inner(s, _):
@@ -477,7 +492,7 @@
     si = lax.broadcasted_iota(jnp.int32, (256, 384), 1) - 128
     band = jnp.where((si <= ti) & (si > ti - span) & (si >= -16), 1.0, 0.0).astype(BF16)
     position = here * 256 + lax.broadcasted_iota(jnp.int32, (256, 128), 0)
-    amount = jnp.minimum(position + 1, span).astype(F32)
+    inverse = 1.0 / jnp.minimum(position + 1, span).astype(F32)
 
     def pool(s, _):
         EXT[s, 0:128, :] = jnp.zeros((128, 128), BF16)
@@ -487,22 +502,22 @@
             EXT[s, 112:128, :] = BR[s]
 
         window = dot(band, EXT[s])
-        PO[s] = (window / amount - EXT[s, 128:384, :].astype(F32)).astype(BF16)
+        PO[s] = (window * inverse - EXT[s, 128:384, :].astype(F32)).astype(BF16)
         return 0
 
-    def give_back(buffer, slot):
-        n = sem()
-        ACT[slot + f] = buffer[f]
-        for k in (1, 3, 2):
-            send(n, buffer.at[fat(k)], ACT.at[slot + f], {"fs": fat(k)})
-        return n
-
-    given = []
+    given_pool, given_rec = sem(), sem()
+
+    def give_back(buffer, slot, n, sources):
+        for s in sources:
+            if s == 1:
+                ACT[slot + f] = buffer[1]
+            else:
+                send(n, buffer.at[s], ACT.at[slot + f], {"fs": fat(s - 1)})
 
     def pooling():
         landed(nb, BR)
         each(pool)
-        given.append(give_back(PO, 4))
+        give_back(PO, 4, given_pool, (0, 2, 3, 1))
 
     def pass_z(i, state):
         later, fade = unpack_state(ZR[i])
@@ -526,9 +541,10 @@
             send(sb, ES.at[xat(k)], ER.at[x], {"sp_1": xat(k)})
 
     def finish(s, _):
-        entering = ER[s].astype(F32)
+        sequence = fat(s - 1)
+        entering = ER[sequence].astype(F32)
         middle = jnp.exp(C[s, BLOCK - 1 : BLOCK, :]) * entering + A0[s]
-        for b, state in enumerate((ER[s], middle.astype(BF16))):
+        for b, state in enumerate((ER[sequence], middle.astype(BF16))):
             rows = slice(b * BLOCK, (b + 1) * BLOCK)
             raw = INS[s, rows, :] + dot(QE[s, rows, :], state, NT)
             square = jnp.mean(raw * raw, axis=1, keepdims=True)
@@ -537,8 +553,18 @@
 
     def finishing():
         landed(sb, ER.at[pl.ds(0, 3)])
-        each(finish)
-        given.append(give_back(RO, 0))
+        for s in (0, 2, 3, 1):
+            finish(s, 0)
+            give_back(RO, 0, given_rec, (s,))
+
+    def out_pool():
+        landed(given_pool, ACT.at[pl.ds(4, 3)])
+        parts = [ACT[4 + i] for i in range(4)]
+        b, d = parts[0], jnp.concatenate(parts[1:], axis=1)
+        for i in range(4):
+            at, cols = slice(2 * i, 2 * i + 2), slice(512 * i, 512 * i + 512)
+            total = dot(b, GZ3[at, :, :, 256:].reshape(512, 128), NT)
+            PT[:, cols] = total + dot(d, GB[at].reshape(512, WB), NT)
 
     steps.update(
         SQ=squares_near,
@@ -550,6 +576,7 @@
         POOL=pooling,
         PASSZ=from_z,
         FIN=finishing,
+        OUTP=out_pool,
     )
     order = ORDER
     assert sorted(order) == sorted(steps)
@@ -557,26 +584,22 @@
         with jax.named_scope(step):
             steps[step]()
 
-    for n in given:
-        landed(n, ACT.at[pl.ds(0, 3)])
-
-    a, b, d = (
-        jnp.concatenate([ACT[i] for i in range(*span)], axis=1) for span in ((0, 2), (2, 5), (5, 8))
-    )
+    landed(given_rec, ACT.at[pl.ds(0, 3)])
+
+    a, b = (jnp.concatenate([ACT[i], ACT[i + 1]], axis=1) for i in (0, 2))
     my_rows = pl.ds(pl.multiple_of(c * 128, 128), 128)
     their_rows = pl.ds(pl.multiple_of(other * 128, 128), 128)
     swap = sem()
     for i in range(4):
         at, cols = slice(2 * i, 2 * i + 2), slice(512 * i, 512 * i + 512)
-        total = dot(a, GX3[at].reshape(512, 256), NT)
-        total += dot(b, GZ3[at].reshape(512, WZ[2]), NT)
-        total += dot(d, GB[at].reshape(512, WB), NT)
+        total = PT[:, cols] + dot(a, GX3[at].reshape(512, 256), NT)
+        total += dot(b, GZ3[at, :, :, :256].reshape(512, 256), NT)
         PS[:, cols] = total.astype(BF16)
         send(swap, PS.at[their_rows, pl.ds(512 * i, 512)], PR.at[:, pl.ds(512 * i, 512)], {"tp": other})
     landed(swap, PR)
     out[...] = (PS[my_rows, :].astype(F32) + PR[...].astype(F32)).astype(BF16)
 
-    for made in sent[-NSEND:]:
+    for made in sent[-NSEND:] + sent_long[-NLONG:]:
         made.wait_send()
 
     @pl.when(f == x)
@@ -607,7 +630,9 @@
     mixed = pl.pallas_call(
         kernel,
         out_shape=jax.ShapeDtypeStruct((128, 2048), BF16),
-        in_specs=[pl.BlockSpec(memory_space=pltpu.VMEM)] * 15,
+        in_specs=[
+            pl.BlockSpec(memory_space=pl.ANY if i in (0, 10, 11) else pltpu.VMEM) for i in range(15)
+        ],
         out_specs=pl.BlockSpec(memory_space=pltpu.VMEM),
         scratch_shapes=[
             half(2, 4, 256, 1024),
@@ -643,12 +668,16 @@
             half(128, 2048),
             vmem(4, 256, 1),
             half(4, 128, 128),
+            vmem(4, 128, 128),
+            half(2, 256, 256),
+            vmem(256, 2048),
             half(4, 16, 256),
             half(4, 16, 256),
             half(4, 16, 128),
             half(16, 640),
-            pltpu.SemaphoreType.DMA((NSEND + 3,)),
+            pltpu.SemaphoreType.DMA((NSEND + NLONG + 3,)),
             pltpu.SemaphoreType.DMA((NRECV,)),
+            pltpu.SemaphoreType.DMA((3,)),
         ],
         compiler_params=pltpu.CompilerParams(
             collective_id=0, has_side_effects=True, vmem_limit_bytes=60 * 1024 * 1024
@@ -662,13 +691,13 @@
         outgate_weight,
         pool_in_weight,
         forget_room.reshape(4, 128),
-        decay_shift[0],
+        decay_shift[0].T,
         head_gain.reshape(1, 128),
         start_state,
         pool_map,
         pool_scale.reshape(1, 512),
-        out_rec_weight,
-        out_pool_weight,
+        out_rec_weight.T,
+        out_pool_weight.T,
     )
     return mixed[None]
 

time: 79.4 us -> 72.8 us (0.917)
  Pallas kernels: 74.3 us -> 70.7 us
  local copies, waits for them, and re-layouts: 4.87 us -> 1.88 us
    pallas_call x1, Pallas kernels: 74.3 us -> 70.7 us  [per_device(): pl.pallas_call(kernel, out_shape=jax.ShapeDtypeStruct((128, 2048), BF16),...]
    unnamed x10 -> x1, local copies, waits for them, and re-layouts: 4.87 us -> 1.88 us
where the time goes in v5:
time: 72.8 us; the launch traced here: 72.6 us
  Pallas kernels  70.7 us (97%)
  local copies, waits for them, and re-layouts  1.88 us (3%)
    pallas_call x1, Pallas kernels, per_device(): pl.pallas_call(kernel, out_shape=jax.ShapeDtypeStruct((128, 2048), BF16),...  70.7 us
    unnamed x1, local copies, waits for them, and re-layouts  1.88 us

profile of v5, /device:TPU:1, one launch (start us, length us, event | category | flops | bytes accessed | tf_op | source)
XLA Modules:
  0.0 72.6 jit_solution(15504802106629074890)
XLA Ops:
  0.0 70.7 %shard_map.145 = bf16[128,2048]{1,0:T(8,128)(2,1)} custom-call(bf16[256,1024]{1,0:T(8,128)(2,1)} %bitcast.12, f32[16,128]{1,0:T(8,128)} %bitcast.15, bf16[16,512]{1,0:T(8,128)(2,1)} %wq.1, bf16[16,512]{1,0:T(8,128)(2,1)} %wf.1, bf16[16,512]{1,0:T(8,128)(2,1)} %wv.1, bf16[16,512]{1,0:T(8,128)(2,1)} %wo.1, bf16[16,512]{1,0:T(8,128)(2,1)} %wp.1, ...), custom_call_target="tpu_custom_call" | custom-call | tf_op jit(solution)/shard_map/pallas_call | solution.py:630
  70.7 1.9 %copy.17 = bf16[1,128,2048]{2,1,0:T(8,128)(2,1)} copy(bf16[1,128,2048]{2,1,0:T(8,128)(2,1)} %bitcast.11) | data formatting | bytes 1048576

commit v6 on v5

--- a/solution.py
+++ b/solution.py
@@ -17,16 +17,16 @@
 EPSILON = 1e-06
 MESH = pl.DeviceIdType.MESH
 ORDER = (
-    "LZ0", "LZ1", "LF0", "1Z0", "LX0", "2Z0", "LZ2", "LF1", "1Z1", "1F0", "1Z2", "2X0", "LF2", "T1",
-    "3Z0", "1Z3", "1Z4", "LX1", "2Z1", "LZ3", "T2", "1F1", "1F2", "2X1", "SQ", "1F3", "LX2", "LZ4",
-    "1F4", "3X0", "3Z1", "LF3", "2Z2", "T3", "LF4", "2X2", "1L", "PR3", "PR1", "2Z3", "3X1", "LX3",
-    "LL", "2X3", "3Z2", "2Z4", "SUMX", "3F0", "2F0", "2F1", "2F2", "2F3", "LX4", "Y0", "3F1", "2F4",
-    "3Z3", "2X4", "3F2", "2L", "REST", "Y1", "3X2", "3F3", "INNER", "PASSZ", "POOL", "3Z4", "3X3",
+    "LZ0", "LZ1", "LF0", "1Z0", "2Z0", "3Z0", "1Z1", "1F0", "LZ2", "LX0", "1Z2", "2X0", "T1", "LF1",
+    "1F1", "1Z3", "1Z4", "LF2", "LZ3", "2F0", "1F2", "LX1", "T2", "2Z1", "2X1", "LZ4", "1F3", "SQ",
+    "1F4", "LX2", "LF3", "3Z1", "2Z2", "3X0", "2X2", "T3", "2F1", "LF4", "LX3", "1L", "PR3", "PR1",
+    "2Z3", "2F2", "LL", "3X1", "2X3", "LX4", "Y0", "2Z4", "3Z2", "SUMX", "3F0", "3F1", "2F3", "2X4",
+    "2F4", "3F2", "Y1", "2L", "REST", "3Z3", "3X2", "INNER", "PASSZ", "POOL", "3Z4", "3F3", "3X3",
     "FIN", "Y2", "3F4", "3X4", "3L", "OUTP",
 )
 NRECV, NSEND, NLONG = 77, 40, 13
 NZ, NX, NF = 8, 4, 4
-WX, WZ, WB, WBX = (256, 256), (256, 128, 384), 384, 128
+WX, WZ, WB, WBX = (128, 256), (256, 256, 256), 512, 256
 F32, BF16 = jnp.float32, jnp.bfloat16
 NT = (((1,), (1,)), ((), ()))
 TN = (((0,), (0,)), ((), ()))
@@ -57,21 +57,21 @@
 
 
 def kernel(
-    tok,
-    gain,
-    wq,
-    wf,
-    wv,
-    wo,
-    wp,
-    room,
-    shift,
-    hgain,
-    start,
-    pmap,
-    pscale,
-    worec,
-    wopool,
+    h_tok,
+    h_gain,
+    h_wq,
+    h_wf,
+    h_wv,
+    h_wo,
+    h_wp,
+    h_room,
+    h_shift,
+    h_hgain,
+    h_start,
+    h_pmap,
+    h_pscale,
+    h_worec,
+    h_wopool,
     out,
     T,
     GZ1,
@@ -109,6 +109,17 @@
     S0,
     PM,
     PT,
+    gain,
+    wq,
+    wf,
+    wv,
+    wo,
+    wp,
+    pscale,
+    worec,
+    wopool,
+    room,
+    hgain,
     iz1,
     ix2,
     iz2,
@@ -129,10 +140,24 @@
     nxt = {"sp_0": after // NX, "sp_1": lax.rem(after, NX)}
     prv = {"sp_0": ahead // NX, "sp_1": lax.rem(ahead, NX)}
 
-    taken = [
-        pltpu.make_async_copy(source, target, local_sems.at[i])
-        for i, (source, target) in enumerate(((pmap, PM), (tok, T.at[c, 1]), (start.at[0], S0)))
-    ]
+    arguments = (
+        (h_gain, gain),
+        (h_wf, wf),
+        (h_wv, wv),
+        (h_wq, wq),
+        (h_wo, wo),
+        (h_wp, wp),
+        (h_pmap, PM),
+        (h_pscale, pscale),
+        (h_worec, worec),
+        (h_wopool, wopool),
+        (h_tok, T.at[c, 1]),
+        (h_shift, SH.at[1]),
+        (h_start.at[0], S0),
+        (h_room, room),
+        (h_hgain, hgain),
+    )
+    taken = [pltpu.make_async_copy(a, b, local_sems.at[i]) for i, (a, b) in enumerate(arguments)]
     for made in taken:
         made.start()
 
@@ -175,30 +200,23 @@
     rank = here * NF + f
     row = lax.broadcasted_iota(jnp.int32, (16, 128), 0)
     lane = lax.broadcasted_iota(jnp.int32, (16, 128), 1)
+    for made in taken[:3]:
+        made.wait()
     gains = jnp.broadcast_to(gain[pl.ds(rank // 8, 1), :], (16, 128))
     gains = jnp.where(lane == lax.rem(rank, 8) * 16 + row, gains, 0.0)
     gains = jnp.sum(gains, axis=1, keepdims=True)
-    taken[0].wait()
-    weights = [(w[...].astype(F32) * gains).astype(BF16) for w in (wf, wv, wq, wo)]
-    folded = [dot(wp[:, 256 * i : 256 * i + 256], PM[i]) for i in range(2)]
-    weights.append((jnp.concatenate(folded, axis=1) * gains * pscale[...]).astype(BF16))
-    turned = jnp.concatenate([worec[...], wopool[...]], axis=1)
-    for i in range(NF):
-        chunk = [w[:, 128 * i : 128 * i + 128] for w in weights]
-        iz1[i] = jnp.concatenate(chunk[:2], axis=1)
-        ix2[i] = jnp.concatenate(chunk[2:4], axis=1)
-        iz2[i] = chunk[4]
-    ixz3[...] = turned[:, :640]
     mine = pl.ds(pl.multiple_of(f * 16, 16), 16)
-    pieces = ((GZ1, iz1), (GX2, ix2), (GZ2, iz2))
-    for buffer, own in pieces:
-        buffer[z, x, mine, :] = own[f]
-    GX3[z, x, mine, :] = turned[:, :256]
-    GZ3[z, x, mine, :] = turned[:, 256:640]
-    GB[z, x, mine, :] = turned[:, 640:]
-    SH[1] = shift[...]
-    taken[1].wait()
-
+
+    def stage(buffer, place, weights):
+        for i in range(NF):
+            chunk = [w[:, 128 * i : 128 * i + 128] for w in weights]
+            buffer[i] = jnp.concatenate(chunk, axis=1)
+        place[z, x, mine, :] = buffer[f]
+
+    def scaled(w):
+        return (w[...].astype(F32) * gains).astype(BF16)
+
+    stage(iz1, GZ1, (scaled(wf), scaled(wv)))
     pl.semaphore_wait(barrier, len(met))
 
     def over_y(pairs):
@@ -214,11 +232,22 @@
         for k in (1, 3, 2):
             to = {"fs": fat(k)}
             send(ns[0], ixz3.at[:, pl.ds(0, 256)], GX3.at[z, x, mine, :], to)
-            send(ns[1], ixz3.at[:, pl.ds(256, 384)], GZ3.at[z, x, mine, :], to)
+            send(ns[1], ixz3.at[:, pl.ds(256, 256)], GZ3.at[z, x, mine, :], to)
         return [(n, b.at[z, x, pl.ds(0, 48), :]) for n, b in zip(ns, (GX3, GZ3))]
 
-    y1 = over_y(pieces[:1])
-    y2 = over_y(pieces[1:3])
+    y1 = over_y(((GZ1, iz1),))
+    for made in taken[3:12]:
+        made.wait()
+    folded = [dot(wp[:, 256 * i : 256 * i + 256], PM[i]) for i in range(2)]
+    folded = (jnp.concatenate(folded, axis=1) * gains * pscale[...]).astype(BF16)
+    turned = jnp.concatenate([worec[...], wopool[...]], axis=1)
+    stage(ix2, GX2, (scaled(wq),))
+    stage(iz2, GZ2, (scaled(wo), folded))
+    ixz3[...] = turned[:, :512]
+    GX3[z, x, mine, :] = turned[:, :256]
+    GZ3[z, x, mine, :] = turned[:, 256:512]
+    GB[z, x, mine, :] = turned[:, 512:]
+    y2 = over_y(((GX2, ix2), (GZ2, iz2)))
     y3 = over_out()
     nshift = sem()
     for k in (1, 3, 2):
@@ -327,7 +356,7 @@
 
         return (GX is not None) and (lambda zi, xi: GX.at[zi, xi]), vz
 
-    lanes = (pl.ds(WBX, WB - WBX), pl.ds(WBX, 128), pl.ds(WBX + 128, 128))
+    lanes = (pl.ds(WBX, 256), pl.ds(WBX, 128), pl.ds(WBX + 128, 128))
     plane(
         "L",
         (),
@@ -365,7 +394,8 @@
     def start_copies():
         return [copy(ns, SS.at[fat(k)], ST, {"fs": fat(k)}, NSEND + NLONG + i) for i, k in enumerate((1, 2, 3))]
 
-    taken[2].wait()
+    for made in taken[12:]:
+        made.wait()
 
     @pl.when(f == x)
     def _():
@@ -384,7 +414,6 @@
     i1 = lax.broadcasted_iota(jnp.int32, (BLOCK, BLOCK), 1)
     causal = i0 >= i1
     tril = jnp.where(causal, 1.0, 0.0).astype(BF16)
-    ones = jnp.ones((BLOCK, BLOCK), BF16)
     my_room = room[pl.ds(f, 1), :]
 
     half = NZ // 2
@@ -402,28 +431,36 @@
         total = total * SC[at].reshape(count, 1)
         return [total[256 * i : 256 * i + 256] for i in range(len(slots))]
 
-    def project(s, both):
-        keys = my_room * jax.nn.sigmoid(-both[:, :128])
-        K[s] = keys
-        value = both[:, 128:].astype(BF16)
-        V[s] = value
-        lag = SH[s, pl.ds(f, 1), :]
-        ends, adds = [], []
-        for b in range(2):
-            rows = slice(b * BLOCK, (b + 1) * BLOCK)
-            lags = three_parts(lag[:, rows])
-            spread = [jnp.where(causal, jnp.broadcast_to(p, (BLOCK, BLOCK)), 0.0).astype(BF16) for p in lags]
-            parts = [p.astype(BF16) for p in three_parts(jnp.log1p(-keys[rows]))]
-            within = dot(
-                jnp.concatenate([tril] * 3 + spread, axis=1),
-                jnp.concatenate(parts + [ones] * 3, axis=0),
-            )
-            C[s, rows, :] = within
-            end = within[BLOCK - 1 :]
-            adds.append(dot(value[rows], (keys[rows] * jnp.exp(end - within)).astype(BF16), TN))
-            ends.append(end)
-        A0[s] = adds[0]
-        SL[s] = pack_state(jnp.exp(ends[1]) * adds[0] + adds[1], ends[0] + ends[1])
+    def project(slots):
+        keys, values, parts, spread = [], [], [], []
+        halves = (slice(0, BLOCK), slice(BLOCK, 2 * BLOCK))
+        for s, both in zip(slots, through(slots, GZ1)):
+            keys.append(my_room * jax.nn.sigmoid(-both[:, :128]))
+            values.append(both[:, 128:].astype(BF16))
+            K[s], V[s] = keys[-1], values[-1]
+        for s, key in zip(slots, keys):
+            logs = [p.astype(BF16) for p in three_parts(jnp.log1p(-key))]
+            lags = three_parts(SH[s, pl.ds(f, 1), :])
+            for rows in halves:
+                parts.append(jnp.concatenate([p[rows] for p in logs], axis=0))
+                masked = [jnp.broadcast_to(p[:, rows], (BLOCK, BLOCK)) for p in lags]
+                masked = [jnp.where(causal, p, 0.0).astype(BF16) for p in masked]
+                spread.append(jnp.concatenate(masked, axis=1))
+        within = dot(jnp.concatenate([tril] * 3, axis=1), jnp.concatenate(parts, axis=1))
+        shifts = dot(jnp.concatenate(spread, axis=0), jnp.ones((3 * BLOCK, BLOCK), BF16))
+        ends, faded = [], []
+        for i in range(2 * len(slots)):
+            block = slice(i * BLOCK, i * BLOCK + BLOCK)
+            total = within[:, block] + shifts[block]
+            s, rows = slots[i // 2], halves[i % 2]
+            C[s, rows, :] = total
+            ends.append(total[BLOCK - 1 :])
+            faded.append((keys[i // 2][rows] * jnp.exp(ends[-1] - total)).astype(BF16))
+        adds = [dot(values[i // 2][halves[i % 2]], k, TN) for i, k in enumerate(faded)]
+        for i, s in enumerate(slots):
+            A0[s] = adds[2 * i]
+            state = jnp.exp(ends[2 * i + 1]) * adds[2 * i] + adds[2 * i + 1]
+            SL[s] = pack_state(state, ends[2 * i] + ends[2 * i + 1])
 
     sx, sz, sb, nb = sem(), sem(), sem(), sem()
 
@@ -434,13 +471,12 @@
 
     def project_near():
         landed(nshift, SH.at[pl.ds(0, 3)])
-        for s, both in enumerate(through((0, 1, 2), GZ1)):
-            project(s, both)
+        project((0, 1, 2))
 
     def project_far():
         landed(far_off, T.at[other, 3])
         squares(3)
-        project(3, through((3,), GZ1)[0])
+        project((3,))
         slot_of = lambda sequence: lax.rem(sequence - f + (NF + 1), NF)
         SR[x] = SL[slot_of(x)]
         for k in (1, 3, 2):
@@ -540,31 +576,25 @@
         for k in (1, 3, 2):
             send(sb, ES.at[xat(k)], ER.at[x], {"sp_1": xat(k)})
 
-    def finish(s, _):
-        sequence = fat(s - 1)
-        entering = ER[sequence].astype(F32)
-        middle = jnp.exp(C[s, BLOCK - 1 : BLOCK, :]) * entering + A0[s]
-        for b, state in enumerate((ER[sequence], middle.astype(BF16))):
-            rows = slice(b * BLOCK, (b + 1) * BLOCK)
-            raw = INS[s, rows, :] + dot(QE[s, rows, :], state, NT)
-            square = jnp.mean(raw * raw, axis=1, keepdims=True)
-            RO[s, rows, :] = (raw * lax.rsqrt(square + EPSILON) * G[s, rows, :]).astype(BF16)
-        return 0
-
     def finishing():
         landed(sb, ER.at[pl.ds(0, 3)])
-        for s in (0, 2, 3, 1):
-            finish(s, 0)
+        raws, order = {}, (3, 0, 2, 1)
+        for s in order:
+            entering = ER[fat(s - 1)]
+            middle = jnp.exp(C[s, BLOCK - 1 : BLOCK, :]) * entering.astype(F32) + A0[s]
+            carried = [dot(QE[s, :BLOCK, :], entering, NT), dot(QE[s, BLOCK:, :], middle.astype(BF16), NT)]
+            raws[s] = INS[s] + jnp.concatenate(carried, axis=0)
+        for s in order:
+            square = jnp.mean(raws[s] * raws[s], axis=1, keepdims=True)
+            RO[s] = (raws[s] * lax.rsqrt(square + EPSILON) * G[s]).astype(BF16)
             give_back(RO, 0, given_rec, (s,))
 
     def out_pool():
         landed(given_pool, ACT.at[pl.ds(4, 3)])
-        parts = [ACT[4 + i] for i in range(4)]
-        b, d = parts[0], jnp.concatenate(parts[1:], axis=1)
+        act = jnp.concatenate([ACT[4 + i] for i in range(4)], axis=1)
         for i in range(4):
             at, cols = slice(2 * i, 2 * i + 2), slice(512 * i, 512 * i + 512)
-            total = dot(b, GZ3[at, :, :, 256:].reshape(512, 128), NT)
-            PT[:, cols] = total + dot(d, GB[at].reshape(512, WB), NT)
+            PT[:, cols] = dot(act, GB[at].reshape(512, WB), NT)
 
     steps.update(
         SQ=squares_near,
@@ -586,14 +616,14 @@
 
     landed(given_rec, ACT.at[pl.ds(0, 3)])
 
-    a, b = (jnp.concatenate([ACT[i], ACT[i + 1]], axis=1) for i in (0, 2))
+    act = jnp.concatenate([ACT[i] for i in range(4)], axis=1)
     my_rows = pl.ds(pl.multiple_of(c * 128, 128), 128)
     their_rows = pl.ds(pl.multiple_of(other * 128, 128), 128)
     swap = sem()
     for i in range(4):
         at, cols = slice(2 * i, 2 * i + 2), slice(512 * i, 512 * i + 512)
-        total = PT[:, cols] + dot(a, GX3[at].reshape(512, 256), NT)
-        total += dot(b, GZ3[at, :, :, :256].reshape(512, 256), NT)
+        weight = [w[at].reshape(512, w.shape[-1]) for w in (GX3, GZ3)]
+        total = PT[:, cols] + dot(act, jnp.concatenate(weight, axis=1), NT)
         PS[:, cols] = total.astype(BF16)
         send(swap, PS.at[their_rows, pl.ds(512 * i, 512)], PR.at[:, pl.ds(512 * i, 512)], {"tp": other})
     landed(swap, PR)
@@ -630,9 +660,7 @@
     mixed = pl.pallas_call(
         kernel,
         out_shape=jax.ShapeDtypeStruct((128, 2048), BF16),
-        in_specs=[
-            pl.BlockSpec(memory_space=pl.ANY if i in (0, 10, 11) else pltpu.VMEM) for i in range(15)
-        ],
+        in_specs=[pl.BlockSpec(memory_space=pltpu.HBM)] * 15,
         out_specs=pl.BlockSpec(memory_space=pltpu.VMEM),
         scratch_shapes=[
             half(2, 4, 256, 1024),
@@ -671,13 +699,19 @@
             vmem(4, 128, 128),
             half(2, 256, 256),
             vmem(256, 2048),
-            half(4, 16, 256),
+            vmem(16, 128),
+            *[half(16, 512)] * 5,
+            vmem(1, 512),
+            *[half(16, 512)] * 2,
+            vmem(4, 128),
+            vmem(1, 128),
             half(4, 16, 256),
             half(4, 16, 128),
-            half(16, 640),
+            half(4, 16, 256),
+            half(16, 512),
             pltpu.SemaphoreType.DMA((NSEND + NLONG + 3,)),
             pltpu.SemaphoreType.DMA((NRECV,)),
-            pltpu.SemaphoreType.DMA((3,)),
+            pltpu.SemaphoreType.DMA((15,)),
         ],
         compiler_params=pltpu.CompilerParams(
             collective_id=0, has_side_effects=True, vmem_limit_bytes=60 * 1024 * 1024

time: 72.8 us -> 70.8 us (0.973)
  Pallas kernels: 70.7 us -> 68.8 us
    pallas_call x1, Pallas kernels: 70.7 us -> 68.8 us  [per_device(): pl.pallas_call(kernel, out_shape=jax.ShapeDtypeStruct((128, 2048), BF16),...]
where the time goes in v6:
time: 70.8 us; the launch traced here: 70.7 us
  Pallas kernels  68.8 us (97%)
  local copies, waits for them, and re-layouts  1.88 us (3%)
    pallas_call x1, Pallas kernels, per_device(): pl.pallas_call(kernel, out_shape=jax.ShapeDtypeStruct((128, 2048), BF16),...  68.8 us
    unnamed x1, local copies, waits for them, and re-layouts  1.88 us

profile of v6, /device:TPU:1, one launch (start us, length us, event | category | flops | bytes accessed | tf_op | source)
XLA Modules:
  0.0 70.7 jit_solution(21877985512682230)
XLA Ops:
  0.0 68.8 %shard_map.145 = bf16[128,2048]{1,0:T(8,128)(2,1)} custom-call(bf16[256,1024]{1,0:T(8,128)(2,1)} %bitcast.12, f32[16,128]{1,0:T(8,128)} %bitcast.15, bf16[16,512]{1,0:T(8,128)(2,1)} %h_wq.1, bf16[16,512]{1,0:T(8,128)(2,1)} %h_wf.1, bf16[16,512]{1,0:T(8,128)(2,1)} %h_wv.1, bf16[16,512]{1,0:T(8,128)(2,1)} %h_wo.1, bf16[16,512]{1,0:T(8,128)(2,1)} %h_wp.1, ...), custom_call_target="tpu_custom_call" | custom-call | tf_op jit(solution)/shard_map/pallas_call | solution.py:660
  68.8 1.9 %copy.17 = bf16[1,128,2048]{2,1,0:T(8,128)(2,1)} copy(bf16[1,128,2048]{2,1,0:T(8,128)(2,1)} %bitcast.11) | data formatting | bytes 1048576

commit v7 on v6

--- a/solution.py
+++ b/solution.py
@@ -17,12 +17,81 @@
 EPSILON = 1e-06
 MESH = pl.DeviceIdType.MESH
 ORDER = (
-    "LZ0", "LZ1", "LF0", "1Z0", "2Z0", "3Z0", "1Z1", "1F0", "LZ2", "LX0", "1Z2", "2X0", "T1", "LF1",
-    "1F1", "1Z3", "1Z4", "LF2", "LZ3", "2F0", "1F2", "LX1", "T2", "2Z1", "2X1", "LZ4", "1F3", "SQ",
-    "1F4", "LX2", "LF3", "3Z1", "2Z2", "3X0", "2X2", "T3", "2F1", "LF4", "LX3", "1L", "PR3", "PR1",
-    "2Z3", "2F2", "LL", "3X1", "2X3", "LX4", "Y0", "2Z4", "3Z2", "SUMX", "3F0", "3F1", "2F3", "2X4",
-    "2F4", "3F2", "Y1", "2L", "REST", "3Z3", "3X2", "INNER", "PASSZ", "POOL", "3Z4", "3F3", "3X3",
-    "FIN", "Y2", "3F4", "3X4", "3L", "OUTP",
+    "LZ0",
+    "LZ1",
+    "LF0",
+    "1Z0",
+    "LX0",
+    "3Z0",
+    "LZ2",
+    "LF1",
+    "2Z0",
+    "1Z1",
+    "1Z2",
+    "LF2",
+    "T1",
+    "2X0",
+    "1F0",
+    "1Z3",
+    "1Z4",
+    "LX1",
+    "1F1",
+    "LZ3",
+    "2Z1",
+    "1F2",
+    "2X1",
+    "T2",
+    "LX2",
+    "LZ4",
+    "1F3",
+    "3X0",
+    "1F4",
+    "2F0",
+    "SQ",
+    "2Z2",
+    "LF3",
+    "2F1",
+    "LX3",
+    "LF4",
+    "3Z1",
+    "T3",
+    "1L",
+    "PR3",
+    "PR1",
+    "2Z3",
+    "2X2",
+    "LX4",
+    "LL",
+    "Y0",
+    "2F2",
+    "3X1",
+    "2Z4",
+    "3Z2",
+    "2X3",
+    "SUMX",
+    "2F3",
+    "3F0",
+    "3F1",
+    "2F4",
+    "3Z3",
+    "Y1",
+    "3F2",
+    "2L",
+    "2X4",
+    "REST",
+    "3X2",
+    "3F3",
+    "INNER",
+    "PASSZ",
+    "3Z4",
+    "POOL",
+    "3X3",
+    "FIN",
+    "3F4",
+    "Y2",
+    "3X4",
+    "OUTP",
+    "3L",
 )
 NRECV, NSEND, NLONG = 77, 40, 13
 NZ, NX, NF = 8, 4, 4

time: 70.8 us -> 68.2 us (0.963)
  Pallas kernels: 68.8 us -> 66.2 us
    pallas_call x1, Pallas kernels: 68.8 us -> 66.2 us  [per_device(): pl.pallas_call(kernel, out_shape=jax.ShapeDtypeStruct((128, 2048), BF16),...]
where the time goes in v7:
time: 68.2 us; the launch traced here: 68.1 us
  Pallas kernels  66.2 us (97%)
  local copies, waits for them, and re-layouts  1.88 us (3%)
    pallas_call x1, Pallas kernels, per_device(): pl.pallas_call(kernel, out_shape=jax.ShapeDtypeStruct((128, 2048), BF16),...  66.2 us
    unnamed x1, local copies, waits for them, and re-layouts  1.88 us

profile of v7, /device:TPU:1, one launch (start us, length us, event | category | flops | bytes accessed | tf_op | source)
XLA Modules:
  0.0 68.1 jit_solution(14976799841884632484)
XLA Ops:
  0.0 66.2 %shard_map.145 = bf16[128,2048]{1,0:T(8,128)(2,1)} custom-call(bf16[256,1024]{1,0:T(8,128)(2,1)} %bitcast.12, f32[16,128]{1,0:T(8,128)} %bitcast.15, bf16[16,512]{1,0:T(8,128)(2,1)} %h_wq.1, bf16[16,512]{1,0:T(8,128)(2,1)} %h_wf.1, bf16[16,512]{1,0:T(8,128)(2,1)} %h_wv.1, bf16[16,512]{1,0:T(8,128)(2,1)} %h_wo.1, bf16[16,512]{1,0:T(8,128)(2,1)} %h_wp.1, ...), custom_call_target="tpu_custom_call" | custom-call | tf_op jit(solution)/shard_map/pallas_call | solution.py:729
  66.2 1.9 %copy.17 = bf16[1,128,2048]{2,1,0:T(8,128)(2,1)} copy(bf16[1,128,2048]{2,1,0:T(8,128)(2,1)} %bitcast.11) | data formatting | bytes 1048576

commit v8 on v7

--- a/solution.py
+++ b/solution.py
@@ -783,9 +783,10 @@
             pltpu.SemaphoreType.DMA((15,)),
         ],
         compiler_params=pltpu.CompilerParams(
-            collective_id=0, has_side_effects=True, vmem_limit_bytes=60 * 1024 * 1024
+            collective_id=0, has_side_effects=True, vmem_limit_bytes=48 * 1024 * 1024
         ),
     )(
+        *[pltpu.with_memory_space_constraint(a, pltpu.HBM) for a in (
         tokens[0],
         norm_gain.reshape(16, 128),
         query_weight,
@@ -801,6 +802,7 @@
         pool_scale.reshape(1, 512),
         out_rec_weight.T,
         out_pool_weight.T,
+    )]
     )
     return mixed[None]
 

time: 68.2 us -> 66.4 us (0.974)
  local copies, waits for them, and re-layouts: 1.88 us -> 0.8 us
  Pallas kernels: 66.2 us -> 65.4 us
    unnamed x1, local copies, waits for them, and re-layouts: 1.88 us -> 0.8 us
    pallas_call x1, Pallas kernels: 66.2 us -> 65.4 us  [per_device(): pl.pallas_call(kernel, out_shape=jax.ShapeDtypeStruct((128, 2048), BF16),...]
where the time goes in v8:
time: 66.4 us; the launch traced here: 66.2 us
  Pallas kernels  65.4 us (98%)
  local copies, waits for them, and re-layouts  0.8 us (1%)
    pallas_call x1, Pallas kernels, per_device(): pl.pallas_call(kernel, out_shape=jax.ShapeDtypeStruct((128, 2048), BF16),...  65.4 us

profile of v8, /device:TPU:1, one launch (start us, length us, event | category | flops | bytes accessed | tf_op | source)
XLA Modules:
  0.0 66.2 jit_solution(12524156592665965260)
XLA Ops:
  0.0 65.4 %shard_map.145 = bf16[128,2048]{1,0:T(8,128)(2,1)S(1)} custom-call(bf16[256,1024]{1,0:T(8,128)(2,1)} %bitcast.12, f32[16,128]{1,0:T(8,128)} %bitcast.15, bf16[16,512]{1,0:T(8,128)(2,1)} %h_wq.1, bf16[16,512]{1,0:T(8,128)(2,1)} %h_wf.1, bf16[16,512]{1,0:T(8,128)(2,1)} %h_wv.1, bf16[16,512]{1,0:T(8,128)(2,1)} %h_wo.1, bf16[16,512]{1,0:T(8,128)(2,1)} %h_wp.1, ...), custom_call_target="tpu_custom_call" | custom-call | tf_op jit(solution)/shard_map/pallas_call | solution.py:729
  65.4 0.8 %copy.17 = bf16[1,128,2048]{2,1,0:T(8,128)(2,1)} copy(bf16[1,128,2048]{2,1,0:T(8,128)(2,1)S(1)} %bitcast.11) | data formatting | bytes 1048576

commit v9 on v8

--- a/solution.py
+++ b/solution.py
@@ -81,8 +81,8 @@
     "REST",
     "3X2",
     "3F3",
+    "PASSZ",
     "INNER",
-    "PASSZ",
     "3Z4",
     "POOL",
     "3X3",
@@ -255,10 +255,17 @@
             device_id_type=MESH,
         )
 
+    waited = set()
+
+    def finish_send(made):
+        if id(made) not in waited:
+            waited.add(id(made))
+            made.wait_send()
+
     def send(n, src, dst, who, long=False):
         made_before, slots, base = (sent_long, NLONG, NSEND) if long else (sent, NSEND, 0)
         if len(made_before) >= slots:
-            made_before[-slots].wait_send()
+            finish_send(made_before[-slots])
         made = copy(n, src, dst, who, base + len(made_before) % slots)
         made.start()
         made_before.append(made)
@@ -683,6 +690,8 @@
         with jax.named_scope(step):
             steps[step]()
 
+    for made in sent[-NSEND:-12] + sent_long[-NLONG:]:
+        finish_send(made)
     landed(given_rec, ACT.at[pl.ds(0, 3)])
 
     act = jnp.concatenate([ACT[i] for i in range(4)], axis=1)
@@ -699,7 +708,7 @@
     out[...] = (PS[my_rows, :].astype(F32) + PR[...].astype(F32)).astype(BF16)
 
     for made in sent[-NSEND:] + sent_long[-NLONG:]:
-        made.wait_send()
+        finish_send(made)
 
     @pl.when(f == x)
     def _():

time: 66.4 us -> 65.9 us (level)
  no operation moved by 1% of the time
where the time goes in v9:
time: 65.9 us; the launch traced here: 65.8 us
  Pallas kernels  65 us (99%)
  local copies, waits for them, and re-layouts  0.8 us (1%)
    pallas_call x1, Pallas kernels, per_device(): pl.pallas_call(kernel, out_shape=jax.ShapeDtypeStruct((128, 2048), BF16),...  65 us

profile of v9, /device:TPU:1, one launch (start us, length us, event | category | flops | bytes accessed | tf_op | source)
XLA Modules:
  0.0 65.8 jit_solution(14329820718816444984)
XLA Ops:
  0.0 65.0 %shard_map.145 = bf16[128,2048]{1,0:T(8,128)(2,1)S(1)} custom-call(bf16[256,1024]{1,0:T(8,128)(2,1)} %bitcast.12, f32[16,128]{1,0:T(8,128)} %bitcast.15, bf16[16,512]{1,0:T(8,128)(2,1)} %h_wq.1, bf16[16,512]{1,0:T(8,128)(2,1)} %h_wf.1, bf16[16,512]{1,0:T(8,128)(2,1)} %h_wv.1, bf16[16,512]{1,0:T(8,128)(2,1)} %h_wo.1, bf16[16,512]{1,0:T(8,128)(2,1)} %h_wp.1, ...), custom_call_target="tpu_custom_call" | custom-call | tf_op jit(solution)/shard_map/pallas_call | solution.py:738
  65.0 0.8 %copy.17 = bf16[1,128,2048]{2,1,0:T(8,128)(2,1)} copy(bf16[1,128,2048]{2,1,0:T(8,128)(2,1)S(1)} %bitcast.11) | data formatting | bytes 1048576

commit v10 on v9

--- a/solution.py
+++ b/solution.py
@@ -504,6 +504,8 @@
         low = jnp.concatenate([w[:half].reshape(1024, w.shape[-1]) for w in weights], axis=1)
         high = jnp.concatenate([w[half:].reshape(1024, w.shape[-1]) for w in weights], axis=1)
         total = dot(T[0, at].reshape(count, 1024), low) + dot(T[1, at].reshape(count, 1024), high)
+        if slots == (3,):
+            squares(3)
         total = total * SC[at].reshape(count, 1)
         return [total[256 * i : 256 * i + 256] for i in range(len(slots))]
 
@@ -551,7 +553,6 @@
 
     def project_far():
         landed(far_off, T.at[other, 3])
-        squares(3)
         project((3,))
         slot_of = lambda sequence: lax.rem(sequence - f + (NF + 1), NF)
         SR[x] = SL[slot_of(x)]

time: 65.9 us -> 65.9 us (level)
  no operation moved by 1% of the time
where the time goes in v10:
time: 65.9 us; the launch traced here: 65.8 us
  Pallas kernels  64.9 us (98%)
  local copies, waits for them, and re-layouts  0.8 us (1%)
    pallas_call x1, Pallas kernels, per_device(): pl.pallas_call(kernel, out_shape=jax.ShapeDtypeStruct((128, 2048), BF16),...  64.9 us

profile of v10, /device:TPU:1, one launch (start us, length us, event | category | flops | bytes accessed | tf_op | source)
XLA Modules:
  0.0 65.8 jit_solution(2951973245447940545)
XLA Ops:
  0.0 64.9 %shard_map.145 = bf16[128,2048]{1,0:T(8,128)(2,1)S(1)} custom-call(bf16[256,1024]{1,0:T(8,128)(2,1)} %bitcast.12, f32[16,128]{1,0:T(8,128)} %bitcast.15, bf16[16,512]{1,0:T(8,128)(2,1)} %h_wq.1, bf16[16,512]{1,0:T(8,128)(2,1)} %h_wf.1, bf16[16,512]{1,0:T(8,128)(2,1)} %h_wv.1, bf16[16,512]{1,0:T(8,128)(2,1)} %h_wo.1, bf16[16,512]{1,0:T(8,128)(2,1)} %h_wp.1, ...), custom_call_target="tpu_custom_call" | custom-call | tf_op jit(solution)/shard_map/pallas_call | solution.py:739
  65.0 0.8 %copy.17 = bf16[1,128,2048]{2,1,0:T(8,128)(2,1)} copy(bf16[1,128,2048]{2,1,0:T(8,128)(2,1)S(1)} %bitcast.11) | data formatting | bytes 1048576
